TPU v7x, 32 devices: a whole 2x2x4 slice. The times are simulated.
32 devices in a mesh: sp: 8 (over z, y), tp: 4 (over x, core).
Axes of the slice: x: 2, y: 2, z: 4, core: 2. Of those that a mesh axis runs over, the one named last changes fastest.
Arguments:
- tokens: bfloat16 [4096, 2048], P(('sp', 'tp')), may hold values from -6 to 6
- norm_gain: float32 [2048], replicated, may hold values from 0.1 to 1.9
- query_weight: bfloat16 [2048, 2048], P('sp', 'tp'), may hold values from -0.125 to 0.125
- key_weight: bfloat16 [2048, 2048], P('sp', 'tp'), may hold values from -0.125 to 0.125
- value_weight: bfloat16 [2048, 4096], P('sp', 'tp'), may hold values from -0.125 to 0.125
- retain_gate: bfloat16 [2048, 4096], P('sp', 'tp'), may hold values from -0.125 to 0.125
- unit_value: bfloat16 [2048, 2048], P('sp', 'tp'), may hold values from -0.125 to 0.125
- unit_gate: bfloat16 [2048, 2048], P('sp', 'tp'), may hold values from -0.125 to 0.125
- convolve_gate: bfloat16 [2048, 2048], P('sp', 'tp'), may hold values from -0.125 to 0.125
- filter_taps: float32 [31, 2048], replicated, may hold values from -1 to 1
- layer_gain: float32 [2048], replicated, may hold values from 0.1 to 1.9
- layer_shift: float32 [2048], replicated, may hold values from -3 to 3
- retain_output: bfloat16 [2048, 4096], P('sp', 'tp'), may hold values from -0.09375 to 0.09375
- convolve_output: bfloat16 [2048, 2048], P('sp', 'tp'), may hold values from -0.125 to 0.125
Outputs:
- mixed: bfloat16 [4096, 2048], P(('sp', 'tp'))
All inputs are finite; a program needn't handle non-finite values.
Results may differ from a plain program's by a relative error of at most 0.018.
Values may be sent and summed in bfloat16 or wider, within the bound.
A program may use at most 128 MiB of HBM per device.

v0:
```python
import jax
import jax.numpy as jnp
from jax import lax
from jax.sharding import PartitionSpec as P

KEY = 256
VAL = 512
GROUP = 512
KW = 31


rms_eps = 1e-06
group_eps = 1.0
layer_eps = 0.001
rope_base = 10000.0
highest = lax.Precision.HIGHEST


def carried_in(part, axis, combine, identity):
    place = lax.axis_index(axis)
    gathered = jax.tree.map(lambda a: lax.all_gather(a, axis), part)
    state = jax.tree.map(lambda a, e: jnp.zeros_like(a) + jnp.asarray(e, a.dtype), part, identity)

    def one(hop, state):
        return combine(
            state, jax.tree.map(lambda a: lax.dynamic_index_in_dim(a, hop, 0, False), gathered)
        )

    return lax.fori_loop(0, place, one, state)


def from_behind(x, axis, by):
    length = lax.axis_size(axis)
    pairs = [(i, i + by) for i in range(length) if 0 <= i + by < length]
    return lax.ppermute(x, axis, pairs)


def rms_normalize(tokens, norm_gain):
    widened = tokens.astype(jnp.float32)
    scaled = widened * lax.rsqrt(jnp.mean(widened * widened, axis=-1, keepdims=True) + rms_eps)
    return (scaled * norm_gain).astype(jnp.bfloat16)


def rotate(vectors, positions):
    half_width = vectors.shape[-1] // 2
    frequency = rope_base ** (-jnp.arange(half_width, dtype=jnp.float32) / half_width)
    angles = positions.astype(jnp.float32)[:, None] * frequency
    cosine = jnp.cos(angles)[:, None, :]
    sine_part = jnp.sin(angles)[:, None, :]
    front_half = vectors[..., :half_width]
    back_half = vectors[..., half_width:]
    return jnp.concatenate(
        [front_half * cosine - back_half * sine_part, front_half * sine_part + back_half * cosine],
        axis=-1,
    )


def prepare(queries, key_rows, values, positions):
    row_count = queries.shape[0]
    rotated_query = rotate(
        queries.astype(jnp.float32).reshape(row_count, -1, KEY), positions
    ).astype(jnp.bfloat16)
    rotated_keys = (
        rotate(key_rows.astype(jnp.float32).reshape(row_count, -1, KEY), positions) * KEY ** (-0.5)
    ).astype(jnp.bfloat16)
    value_heads = values.reshape(row_count, -1, VAL)
    return (rotated_query, rotated_keys, value_heads)


def decay_logs(first_head, head_total, all_heads, seq_length):
    ratio = (first_head + jnp.arange(head_total)).astype(jnp.float32) / (all_heads - 1)
    return (jnp.log(0.05) + ratio * jnp.log(18.0)) / seq_length


def local_parts(queries, key_rows, values, log_decay):
    row_count = queries.shape[0]
    indices = jnp.arange(row_count, dtype=jnp.float32)
    offsets = indices[:, None] - indices[None, :]
    causal = offsets >= 0
    weight = jnp.where(
        causal[None], jnp.exp(log_decay[:, None, None] * jnp.where(causal, offsets, 0.0)[None]), 0.0
    )
    scores = (
        jnp.einsum("ihd,jhd->hij", queries, key_rows, preferred_element_type=jnp.float32) * weight
    ).astype(jnp.bfloat16)
    within = jnp.einsum("hij,jhe->ihe", scores, values, preferred_element_type=jnp.float32)
    trailing = jnp.exp(log_decay[None, :] * (row_count - 1.0 - indices)[:, None])
    weighted = (key_rows.astype(jnp.float32) * trailing[:, :, None]).astype(jnp.bfloat16)
    contribution = jnp.einsum("jhd,jhe->hde", weighted, values, preferred_element_type=jnp.float32)
    return (within, contribution)


def cross_part(queries, carry_state, log_decay):
    row_count = queries.shape[0]
    indices = jnp.arange(row_count, dtype=jnp.float32)
    leading = jnp.exp(log_decay[None, :] * (indices + 1.0)[:, None])
    return (
        jnp.einsum("ihd,hde->ihe", queries.astype(jnp.float32), carry_state, precision=highest)
        * leading[:, :, None]
    )


def retain_finish(raw, switch):
    average = jnp.mean(raw, axis=-1, keepdims=True)
    spread = jnp.mean(jnp.square(raw - average), axis=-1, keepdims=True)
    normalized = ((raw - average) * lax.rsqrt(spread + group_eps)).reshape(raw.shape[0], -1)
    return (normalized * jax.nn.silu(switch.astype(jnp.float32))).astype(jnp.bfloat16)


def convolve_branch(gated_input, before, tap_slice, gain_slice, shift_slice, switch):
    padded = jnp.concatenate([before, gated_input], axis=0)
    row_count = gated_input.shape[0]
    summed = jnp.zeros(gated_input.shape, jnp.float32)
    for tap_index in range(tap_slice.shape[0]):
        summed = (
            summed
            + padded[tap_index : tap_index + row_count].astype(jnp.float32) * tap_slice[tap_index]
        )
    grouped = summed.reshape(row_count, -1, GROUP)
    average = jnp.mean(grouped, axis=-1, keepdims=True)
    spread = jnp.mean(jnp.square(grouped - average), axis=-1, keepdims=True)
    normalized = ((grouped - average) * lax.rsqrt(spread + layer_eps)).reshape(row_count, -1)
    normalized = normalized * gain_slice + shift_slice
    return (jax.nn.silu(normalized) * jax.nn.silu(switch.astype(jnp.float32))).astype(jnp.bfloat16)


def contract(hidden, matrix):
    return lax.dot_general(
        hidden, matrix, (((1,), (1,)), ((), ())), preferred_element_type=jnp.float32
    )


def join_states(earlier, later):
    return (earlier[0] * later[0], later[0][:, None, None] * earlier[1] + later[1])


def local(
    tokens,
    norm_gain,
    query_weight,
    key_weight,
    value_weight,
    retain_gate,
    unit_value,
    unit_gate,
    convolve_gate,
    filter_taps,
    layer_gain,
    layer_shift,
    retain_output,
    convolve_output,
):
    head_groups = lax.axis_size("tp")
    chain_length = lax.axis_size("sp")
    head_rank = lax.axis_index("tp")
    chain_rank = lax.axis_index("sp")
    normed = rms_normalize(tokens, norm_gain)
    gathered = (
        lax.all_gather(query_weight, "sp", axis=0, tiled=True),
        lax.all_gather(key_weight, "sp", axis=0, tiled=True),
        lax.all_gather(value_weight, "sp", axis=0, tiled=True),
        lax.all_gather(retain_gate, "sp", axis=0, tiled=True),
        lax.all_gather(unit_value, "sp", axis=0, tiled=True),
        lax.all_gather(unit_gate, "sp", axis=0, tiled=True),
        lax.all_gather(convolve_gate, "sp", axis=0, tiled=True),
        lax.all_gather(retain_output, "sp", axis=0, tiled=True),
        lax.all_gather(convolve_output, "sp", axis=0, tiled=True),
    )
    in_weights = gathered[:7]
    retain_full = gathered[7]
    convolve_full = gathered[8]

    def project(row_piece):
        return jnp.concatenate(
            [
                jnp.dot(row_piece, matrix, preferred_element_type=jnp.float32).astype(jnp.bfloat16)
                for matrix in in_weights
            ],
            axis=1,
        )

    projected = project(lax.all_gather(normed, "tp", axis=0, tiled=True))
    row_count = projected.shape[0]
    bounds = [0]
    for matrix in in_weights:
        bounds.append(bounds[-1] + matrix.shape[1])
    pieces = [projected[:, bounds[column] : bounds[column + 1]] for column in range(7)]
    queries, key_rows, values, retain_switch, glu_value, glu_switch, convolve_switch = pieces
    local_heads = queries.shape[1] // KEY
    positions = chain_rank * row_count + jnp.arange(row_count, dtype=jnp.int32)
    rotated_query, rotated_keys, value_heads = prepare(queries, key_rows, values, positions)
    log_decay = decay_logs(
        head_rank * local_heads, local_heads, local_heads * head_groups, row_count * chain_length
    )
    within, contribution = local_parts(rotated_query, rotated_keys, value_heads, log_decay)
    totals = jnp.exp(log_decay * row_count)
    gated_input = (
        glu_value.astype(jnp.float32) * jax.nn.sigmoid(glu_switch.astype(jnp.float32))
    ).astype(jnp.bfloat16)
    channels = gated_input.shape[1]
    before = from_behind(gated_input[row_count - (KW - 1) :], "sp", 1)
    prefix = carried_in(
        (totals, contribution),
        "sp",
        join_states,
        (jnp.ones_like(totals), jnp.zeros_like(contribution)),
    )
    incoming = prefix[1]
    raw = within + cross_part(rotated_query, incoming, log_decay)
    retain_hidden = retain_finish(raw, retain_switch)
    tap_slice = lax.dynamic_slice_in_dim(filter_taps, head_rank * channels, channels, 1)
    gain_slice = lax.dynamic_slice_in_dim(layer_gain, head_rank * channels, channels, 0)
    shift_slice = lax.dynamic_slice_in_dim(layer_shift, head_rank * channels, channels, 0)
    convolve_hidden = convolve_branch(
        gated_input, before, tap_slice, gain_slice, shift_slice, convolve_switch
    )
    return lax.psum_scatter(
        (contract(retain_hidden, retain_full) + contract(convolve_hidden, convolve_full)).astype(
            jnp.bfloat16
        ),
        "tp",
        scatter_dimension=0,
        tiled=True,
    )


def solution(mesh):
    return jax.shard_map(
        local,
        mesh=mesh,
        in_specs=(
            P(("sp", "tp"), None),
            P(),
            P("sp", "tp"),
            P("sp", "tp"),
            P("sp", "tp"),
            P("sp", "tp"),
            P("sp", "tp"),
            P("sp", "tp"),
            P("sp", "tp"),
            P(),
            P(),
            P(),
            P("sp", "tp"),
            P("sp", "tp"),
        ),
        out_specs=P(("sp", "tp"), None),
        check_vma=False,
    )
```

profile of v0, /device:TPU:2, one launch (start us, length us, event | category | flops | bytes accessed | tf_op | source)
XLA Modules:
  0.0 721.8 jit_solution(9011163686985184079)
XLA Ops:
  7.8 2.0 fusion.17
  13.3 1.8 multiply_cosine_fusion
  15.0 17.6 %all-gather.14.cloned.1.call-done = bf16[512,2048]{1,0:T(8,128)(2,1)} async-done(((bf16[128,2048]{1,0:T(8,128)(2,1)}), bf16[512,2048]{1,0:T(8,128)(2,1)}) %all-gather.14.cloned.1.call-update) | async-done | bytes 2097168 | tf_op jit(solution)/shard_map/all_gather | solution.py:182
  32.7 52.4 %all-gather.18.cloned.1.call-done = bf16[2048,512]{1,0:T(8,128)(2,1)} async-done(((bf16[256,512]{1,0:T(8,128)(2,1)}), bf16[2048,512]{1,0:T(8,128)(2,1)}) %all-gather.18.cloned.1.call-update) | async-done | bytes 2097168 | tf_op jit(solution)/shard_map/all_gather | solution.py:159
  85.0 3.5 convolution_convert_fusion.6
  89.1 45.7 %all-gather.20.cloned.1.call-done = bf16[2048,512]{1,0:T(8,128)(2,1)} async-done(((bf16[256,512]{1,0:T(8,128)(2,1)}), bf16[2048,512]{1,0:T(8,128)(2,1)}) %all-gather.20.cloned.1.call-update) | async-done | bytes 2097168 | tf_op jit(solution)/shard_map/all_gather | solution.py:160
  134.8 3.5 convolution_convert_fusion.5
  138.8 2.0 multiply_subtract_fusion
  140.9 67.3 %all-gather.16.cloned.1.call-done = bf16[2048,1024]{1,0:T(8,128)(2,1)} async-done(((bf16[256,1024]{1,0:T(8,128)(2,1)}), bf16[2048,1024]{1,0:T(8,128)(2,1)}) %all-gather.16.cloned.1.call-update) | async-done | bytes 4194320 | tf_op jit(solution)/shard_map/all_gather | solution.py:161
  208.1 5.1 convolution_convert_fusion.1
  213.3 1.6 fusion.24
  218.3 1.5 constant_dynamic-slice_fusion
  219.8 38.0 %all-gather.26.cloned.1.call-done = bf16[2048,512]{1,0:T(8,128)(2,1)} async-done(((bf16[256,512]{1,0:T(8,128)(2,1)}), bf16[2048,512]{1,0:T(8,128)(2,1)}) %all-gather.26.cloned.1.call-update) | async-done | bytes 2097168 | tf_op jit(solution)/shard_map/all_gather | solution.py:163
  257.8 4.4 fusion.14
  262.2 45.2 %all-gather.28.cloned.1.call-done = bf16[2048,512]{1,0:T(8,128)(2,1)} async-done(((bf16[256,512]{1,0:T(8,128)(2,1)}), bf16[2048,512]{1,0:T(8,128)(2,1)}) %all-gather.28.cloned.1.call-update) | async-done | bytes 2097168 | tf_op jit(solution)/shard_map/all_gather | solution.py:164
  307.4 3.9 fusion.13
  311.3 2.5 collective-permute-start
  313.8 1.7 fusion.89
  315.5 20.4 %all-gather.1 = f32[8,1,2]{2,1,0:T(1,128)} all-gather(f32[1,1,2]{2,1,0:T(1,128)S(1)} %exponential_bitcast_fusion), channel_id=1, replica_groups=mesh['sp'=8,'tp'=4] {'sp'}, dimensions={0}, use_global_device_ids=true | all-gather | bytes 72 | tf_op jit(solution)/shard_map/all_gather | solution.py:21
  337.2 1.3 dynamic_slice.21
  338.6 5.4 fusion.86
  344.2 4.3 fusion.6
  348.5 84.1 %all-gather.34.cloned.1.call-done = f32[16,256,512]{2,1,0:T(8,128)} async-done(((f32[2,256,512]{2,1,0:T(8,128)}), f32[16,256,512]{2,1,0:T(8,128)}) %all-gather.34.cloned.1.call-update) | async-done | bytes 8388624 | tf_op jit(solution)/shard_map/all_gather | solution.py:21
  432.7 3.5 fusion.90
  436.8 1.9 copy.36
  438.7 67.0 %all-gather.22.cloned.1.call-done = bf16[2048,1024]{1,0:T(8,128)(2,1)} async-done(((bf16[256,1024]{1,0:T(8,128)(2,1)}), bf16[2048,1024]{1,0:T(8,128)(2,1)}) %all-gather.22.cloned.1.call-update) | async-done | bytes 4194320 | tf_op jit(solution)/shard_map/all_gather | solution.py:162
  505.7 73.5 %all-gather.24.cloned.1.call-done = bf16[2048,1024]{1,0:T(8,128)(2,1)} async-done(((bf16[256,1024]{1,0:T(8,128)(2,1)}), bf16[2048,1024]{1,0:T(8,128)(2,1)}) %all-gather.24.cloned.1.call-update) | async-done | bytes 4194320 | tf_op jit(solution)/shard_map/all_gather | solution.py:166
  579.2 11.4 %fusion.35 = f32[512,2048]{1,0:T(8,128)} fusion(bf16[2048,1024]{1,0:T(8,128)(2,1)} %all-gather.24.cloned.1.call-done, f32[512,1024]{1,0:T(8,128)} %copy.36, bf16[512,2048]{1,0:T(8,128)(2,1)} %all-gather.14.cloned.1.call-done, bf16[2048,1024]{1,0:T(8,128)(2,1)} %all-gather.22.cloned.1.call-done), kind=kOutput, calls=%fused_computation.89 | convolution fusion | flops 4299161600 | bytes 16777216 | tf_op jit(solution)/shard_map/dot_general | solution.py:128
  590.6 38.3 %all-gather.30.cloned.1.call-done = bf16[2048,512]{1,0:T(8,128)(2,1)} async-done(((bf16[256,512]{1,0:T(8,128)(2,1)}), bf16[2048,512]{1,0:T(8,128)(2,1)}) %all-gather.30.cloned.1.call-update) | async-done | bytes 2097168 | tf_op jit(solution)/shard_map/all_gather | solution.py:165
  628.9 49.8 %all-gather.32.cloned.1.call-done = bf16[2048,512]{1,0:T(8,128)(2,1)} async-done(((bf16[256,512]{1,0:T(8,128)(2,1)}), bf16[2048,512]{1,0:T(8,128)(2,1)}) %all-gather.32.cloned.1.call-update) | async-done | bytes 2097168 | tf_op jit(solution)/shard_map/all_gather | solution.py:167
  678.6 7.6 %add_convert_fusion = bf16[512,2048]{1,0:T(8,128)(2,1)} fusion(f32[512,2048]{1,0:T(8,128)} %fusion.35, bf16[2048,512]{1,0:T(8,128)(2,1)} %all-gather.32.cloned.1.call-done, bf16[512,2048]{1,0:T(8,128)(2,1)S(1)} %copy-done.5, bf16[2048,512]{1,0:T(8,128)(2,1)} %all-gather.30.cloned.1.call-done, f32[512,512]{1,0:T(8,128)S(1)} %get-tuple-element.71, ...), kind=kOutput, calls=%fused_computation.31 | convolution fusion | flops 2153775104 | bytes 13639680 | tf_op jit(solution)/shard_map/dot_general | solution.py:128
  686.2 28.7 %reduce-scatter.2.cloned.1.call-done = bf16[128,2048]{1,0:T(8,128)(2,1)} async-done(((bf16[512,2048]{1,0:T(8,128)(2,1)}), bf16[128,2048]{1,0:T(8,128)(2,1)}) %reduce-scatter.2.cloned.1.call-update) | async-done | bytes 524304 | tf_op jit(solution)/shard_map/reduce_scatter | solution.py:217
  (66 shorter events, 11.1 us)
Async XLA Ops:
  6.5 26.1 %all-gather.14.cloned.1.call-start = ((), (), s32[]{:S(2)}) async-start(), calls=%async_computation.1 | async-start | bytes 2621440 | tf_op jit(solution)/shard_map/all_gather | solution.py:182
  9.8 75.2 %all-gather.18.cloned.1.call-start = ((), (), s32[]{:S(2)}) async-start(), calls=%async_computation.3 | async-start | bytes 2359296 | tf_op jit(solution)/shard_map/all_gather | solution.py:159
  10.6 124.2 %all-gather.20.cloned.1.call-start = ((), (), s32[]{:S(2)}) async-start(), calls=%async_computation.4 | async-start | bytes 2359296 | tf_op jit(solution)/shard_map/all_gather | solution.py:160
  11.3 196.8 %all-gather.16.cloned.1.call-start = ((), (), s32[]{:S(2)}) async-start(), calls=%async_computation.2 | async-start | bytes 4718592 | tf_op jit(solution)/shard_map/all_gather | solution.py:161
  11.9 245.9 %all-gather.26.cloned.1.call-start = ((), (), s32[]{:S(2)}) async-start(), calls=%async_computation.7 | async-start | bytes 2359296 | tf_op jit(solution)/shard_map/all_gather | solution.py:163
  12.5 294.9 %all-gather.28.cloned.1.call-start = ((), (), s32[]{:S(2)}) async-start(), calls=%async_computation.8 | async-start | bytes 2359296 | tf_op jit(solution)/shard_map/all_gather | solution.py:164
  13.1 419.5 %all-gather.34.cloned.1.call-start = ((), (), s32[]{:S(2)}) async-start(), calls=%async_computation.12 | async-start | bytes 9437184 | tf_op jit(solution)/shard_map/all_gather | solution.py:21
  13.1 75.4 %copy-start.4 = (f32[2]{0:T(128)}, f32[2]{0:T(128)S(1)}, u32[]{:S(2)}) copy-start(f32[2]{0:T(128)S(1)} %add_multiply_fusion) | copy-start | bytes 28
  140.9 72.4 %copy-start = (f32[512,2,128]{2,0,1:T(8,128)}, f32[512,2,128]{2,0,1:T(8,128)S(1)}, u32[]{:S(2)}) copy-start(f32[512,2,128]{2,0,1:T(8,128)S(1)} %get-tuple-element.72) | copy-start | bytes 1572868
  140.9 72.4 %copy-start.1 = (f32[512,2,128]{2,0,1:T(8,128)S(1)}, f32[512,2,128]{2,0,1:T(8,128)}, u32[]{:S(2)}) copy-start(f32[512,2,128]{2,0,1:T(8,128)} %get-tuple-element.73) | copy-start | bytes 1572868
  213.3 1.7 copy-start.6
  215.0 290.7 %all-gather.22.cloned.1.call-start = ((), (), s32[]{:S(2)}) async-start(), calls=%async_computation.5 | async-start | bytes 4718592 | tf_op jit(solution)/shard_map/all_gather | solution.py:162
  215.7 363.5 %all-gather.24.cloned.1.call-start = ((), (), s32[]{:S(2)}) async-start(), calls=%async_computation.6 | async-start | bytes 4718592 | tf_op jit(solution)/shard_map/all_gather | solution.py:166
  216.5 412.4 %all-gather.30.cloned.1.call-start = ((), (), s32[]{:S(2)}) async-start(), calls=%async_computation.9 | async-start | bytes 2359296 | tf_op jit(solution)/shard_map/all_gather | solution.py:165
  217.1 461.6 %all-gather.32.cloned.1.call-start = ((), (), s32[]{:S(2)}) async-start(), calls=%async_computation.10 | async-start | bytes 2359296 | tf_op jit(solution)/shard_map/all_gather | solution.py:167
  217.8 497.2 %reduce-scatter.2.cloned.1.call-start = ((), (), s32[]{:S(2)}) async-start(), calls=%async_computation.11 | async-start | bytes 2621440 | tf_op jit(solution)/shard_map/reduce_scatter | solution.py:217
  311.3 27.3 %collective-permute-start = (bf16[30,512]{1,0:T(8,128)(2,1)S(1)}, bf16[30,512]{1,0:T(8,128)(2,1)S(1)}, u32[]{:S(2)}, u32[]{:S(2)}) collective-permute-start(bf16[30,512]{1,0:T(8,128)(2,1)S(1)} %slice.268), channel_id=1, source_target_pairs={{0,4},{4,8},{8,12},{12,16},{16,20},{20,24},{24,28},{1,5},{5,9},{9,... | collective-permute-start | bytes 92168 | tf_op jit(solution)/shard_map/ppermute | solution.py:35
  438.7 239.9 %copy-start.2 = (f32[512]{0:T(512)S(1)}, f32[512]{0:T(512)}, u32[]{:S(2)}) copy-start(f32[512]{0:T(512)} %dynamic_slice.20) | copy-start | bytes 6148
  438.7 239.9 %copy-start.3 = (f32[512]{0:T(512)S(1)}, f32[512]{0:T(512)}, u32[]{:S(2)}) copy-start(f32[512]{0:T(512)} %dynamic_slice.21) | copy-start | bytes 6148
  438.7 239.9 %copy-start.5 = (bf16[512,2048]{1,0:T(8,128)(2,1)S(1)}, bf16[512,2048]{1,0:T(8,128)(2,1)}, u32[]{:S(2)}) copy-start(bf16[512,2048]{1,0:T(8,128)(2,1)} %all-gather.14.cloned.1.call-done) | copy-start | bytes 6291460
Sparse Core Ops, SparseCore 0:
  9.9 22.6 all-gather.13
  34.8 50.1 all-gather.17
  87.1 47.6 all-gather.19
  136.8 71.3 all-gather.15
  210.1 47.6 all-gather.25
  259.7 47.6 all-gather.27
  309.5 123.0 all-gather.33
  434.7 70.9 all-gather.21
  507.9 71.3 all-gather.23
  581.2 47.6 all-gather.29
  631.0 47.5 all-gather.31
  686.3 28.5 reduce-scatter.1
where the time goes:
time: 725 us; the launch traced here: 722 us
  waiting for transfers between devices  613 us (85%)
  matrix products  48.8 us (7%)
  blocking collectives  20.4 us (3%)
  other arithmetic  13.8 us (2%)
  between operations  13.8 us (2%)
  local copies, waits for them, and re-layouts  8.88 us (1%)
    all_gather x1, waiting for transfers between devices, carried_in(): gathered = jax.tree.map(lambda a: lax.all_gather(a, axis), part)  84.1 us
    all_gather x1, waiting for transfers between devices, local(): lax.all_gather(retain_output, 'sp', axis=0, tiled=True)  73.5 us
    all_gather x1, waiting for transfers between devices, local(): lax.all_gather(value_weight, 'sp', axis=0, tiled=True)  67.3 us
    all_gather x1, waiting for transfers between devices, local(): lax.all_gather(retain_gate, 'sp', axis=0, tiled=True)  67 us
    all_gather x1, waiting for transfers between devices, local(): lax.all_gather(query_weight, 'sp', axis=0, tiled=True)  52.4 us
    all_gather x1, waiting for transfers between devices, local(): lax.all_gather(convolve_output, 'sp', axis=0, tiled=True)  49.8 us
    all_gather x1, waiting for transfers between devices, local(): lax.all_gather(key_weight, 'sp', axis=0, tiled=True)  45.7 us
    all_gather x1, waiting for transfers between devices, local(): lax.all_gather(unit_gate, 'sp', axis=0, tiled=True)  45.2 us
  transfers between devices with their start and end apart: 13, of which 12 were waited for; matrix products, arithmetic and copies ran while one was open for 8% of the time, Pallas kernels for 0%

commit v1 on v0

--- a/solution.py
+++ b/solution.py
@@ -1,6 +1,7 @@
 import jax
 import jax.numpy as jnp
 from jax import lax
+from jax.sharding import Mesh
 from jax.sharding import PartitionSpec as P
 
 KEY = 256
@@ -13,26 +14,42 @@
 group_eps = 1.0
 layer_eps = 0.001
 rope_base = 10000.0
-highest = lax.Precision.HIGHEST
-
-
-def carried_in(part, axis, combine, identity):
-    place = lax.axis_index(axis)
-    gathered = jax.tree.map(lambda a: lax.all_gather(a, axis), part)
-    state = jax.tree.map(lambda a, e: jnp.zeros_like(a) + jnp.asarray(e, a.dtype), part, identity)
-
-    def one(hop, state):
-        return combine(
-            state, jax.tree.map(lambda a: lax.dynamic_index_in_dim(a, hop, 0, False), gathered)
-        )
-
-    return lax.fori_loop(0, place, one, state)
-
-
-def from_behind(x, axis, by):
-    length = lax.axis_size(axis)
-    pairs = [(i, i + by) for i in range(length) if 0 <= i + by < length]
-    return lax.ppermute(x, axis, pairs)
+
+
+SPANS = ("tp", "lo")
+
+
+def swap_planes(x):
+    size = lax.axis_size("tp")
+    pairs = [(h * size + t, t * size + h) for h in range(size) for t in range(size)]
+    return lax.ppermute(x, ("hi", "tp"), pairs)
+
+
+def swap_planes_rolled(x):
+    size = lax.axis_size("tp")
+    pairs = [
+        (h * size + t, t * size + (h + size // 2) % size)
+        for h in range(size)
+        for t in range(size)
+    ]
+    return lax.ppermute(x, ("hi", "tp"), pairs)
+
+
+def from_behind(x, by):
+    outer, inner = lax.axis_size("tp"), lax.axis_size("lo")
+    spot = [(i % inner) * outer + i // inner for i in range(outer * inner)]
+    return lax.ppermute(x, ("lo", "tp"), list(zip(spot[:-by], spot[by:])))
+
+
+def carried_in(contribution, log_span_decay):
+    length = lax.axis_size(SPANS)
+    state = from_behind(contribution.astype(jnp.bfloat16), 1).astype(jnp.float32)
+    by = 1
+    while by < length:
+        earlier = from_behind(state.astype(jnp.bfloat16), by).astype(jnp.float32)
+        state = state + jnp.exp(log_span_decay * by)[:, None, None] * earlier
+        by *= 2
+    return state
 
 
 def rms_normalize(tokens, norm_gain):
@@ -95,7 +112,12 @@
     indices = jnp.arange(row_count, dtype=jnp.float32)
     leading = jnp.exp(log_decay[None, :] * (indices + 1.0)[:, None])
     return (
-        jnp.einsum("ihd,hde->ihe", queries.astype(jnp.float32), carry_state, precision=highest)
+        jnp.einsum(
+            "ihd,hde->ihe",
+            queries,
+            carry_state.astype(jnp.bfloat16),
+            preferred_element_type=jnp.float32,
+        )
         * leading[:, :, None]
     )
 
@@ -128,10 +150,6 @@
     return lax.dot_general(
         hidden, matrix, (((1,), (1,)), ((), ())), preferred_element_type=jnp.float32
     )
-
-
-def join_states(earlier, later):
-    return (earlier[0] * later[0], later[0][:, None, None] * earlier[1] + later[1])
 
 
 def local(
@@ -150,42 +168,35 @@
     retain_output,
     convolve_output,
 ):
-    head_groups = lax.axis_size("tp")
-    chain_length = lax.axis_size("sp")
-    head_rank = lax.axis_index("tp")
-    chain_rank = lax.axis_index("sp")
-    normed = rms_normalize(tokens, norm_gain)
-    gathered = (
-        lax.all_gather(query_weight, "sp", axis=0, tiled=True),
-        lax.all_gather(key_weight, "sp", axis=0, tiled=True),
-        lax.all_gather(value_weight, "sp", axis=0, tiled=True),
-        lax.all_gather(retain_gate, "sp", axis=0, tiled=True),
-        lax.all_gather(unit_value, "sp", axis=0, tiled=True),
-        lax.all_gather(unit_gate, "sp", axis=0, tiled=True),
-        lax.all_gather(convolve_gate, "sp", axis=0, tiled=True),
-        lax.all_gather(retain_output, "sp", axis=0, tiled=True),
-        lax.all_gather(convolve_output, "sp", axis=0, tiled=True),
-    )
-    in_weights = gathered[:7]
-    retain_full = gathered[7]
-    convolve_full = gathered[8]
-
-    def project(row_piece):
-        return jnp.concatenate(
-            [
-                jnp.dot(row_piece, matrix, preferred_element_type=jnp.float32).astype(jnp.bfloat16)
-                for matrix in in_weights
-            ],
-            axis=1,
-        )
-
-    projected = project(lax.all_gather(normed, "tp", axis=0, tiled=True))
-    row_count = projected.shape[0]
-    bounds = [0]
-    for matrix in in_weights:
-        bounds.append(bounds[-1] + matrix.shape[1])
-    pieces = [projected[:, bounds[column] : bounds[column + 1]] for column in range(7)]
-    queries, key_rows, values, retain_switch, glu_value, glu_switch, convolve_switch = pieces
+    head_groups = lax.axis_size("hi")
+    chain_length = lax.axis_size(SPANS)
+    head_rank = lax.axis_index("hi")
+    chain_rank = lax.axis_index(SPANS)
+    normed = lax.all_gather(
+        swap_planes(rms_normalize(tokens, norm_gain)), "hi", axis=0, tiled=True
+    )
+    half = normed.shape[1] // 2
+    normed_rolled = jnp.concatenate([normed[:, half:], normed[:, :half]], axis=1)
+
+    def straight(matrix):
+        return lax.all_gather(swap_planes(matrix), SPANS, axis=0, tiled=True)
+
+    def rolled(matrix):
+        return lax.all_gather(swap_planes_rolled(matrix), SPANS, axis=0, tiled=True)
+
+    def project(rows, matrix):
+        return jnp.dot(rows, matrix, preferred_element_type=jnp.float32).astype(jnp.bfloat16)
+
+    key_rows = project(normed, straight(key_weight))
+    values = project(normed_rolled, rolled(value_weight))
+    queries = project(normed, straight(query_weight))
+    glu_value = project(normed, straight(unit_value))
+    glu_switch = project(normed_rolled, rolled(unit_gate))
+    convolve_switch = project(normed, straight(convolve_gate))
+    retain_switch = project(normed_rolled, rolled(retain_gate))
+    convolve_full = rolled(convolve_output)
+    retain_full = straight(retain_output)
+    row_count = normed.shape[0]
     local_heads = queries.shape[1] // KEY
     positions = chain_rank * row_count + jnp.arange(row_count, dtype=jnp.int32)
     rotated_query, rotated_keys, value_heads = prepare(queries, key_rows, values, positions)
@@ -193,19 +204,12 @@
         head_rank * local_heads, local_heads, local_heads * head_groups, row_count * chain_length
     )
     within, contribution = local_parts(rotated_query, rotated_keys, value_heads, log_decay)
-    totals = jnp.exp(log_decay * row_count)
     gated_input = (
         glu_value.astype(jnp.float32) * jax.nn.sigmoid(glu_switch.astype(jnp.float32))
     ).astype(jnp.bfloat16)
     channels = gated_input.shape[1]
-    before = from_behind(gated_input[row_count - (KW - 1) :], "sp", 1)
-    prefix = carried_in(
-        (totals, contribution),
-        "sp",
-        join_states,
-        (jnp.ones_like(totals), jnp.zeros_like(contribution)),
-    )
-    incoming = prefix[1]
+    before = from_behind(gated_input[row_count - (KW - 1) :], 1)
+    incoming = carried_in(contribution, log_decay * row_count)
     raw = within + cross_part(rotated_query, incoming, log_decay)
     retain_hidden = retain_finish(raw, retain_switch)
     tap_slice = lax.dynamic_slice_in_dim(filter_taps, head_rank * channels, channels, 1)
@@ -214,36 +218,34 @@
     convolve_hidden = convolve_branch(
         gated_input, before, tap_slice, gain_slice, shift_slice, convolve_switch
     )
-    return lax.psum_scatter(
-        (contract(retain_hidden, retain_full) + contract(convolve_hidden, convolve_full)).astype(
-            jnp.bfloat16
-        ),
-        "tp",
-        scatter_dimension=0,
-        tiled=True,
-    )
+    convolved_out = contract(convolve_hidden, convolve_full)
+    convolved_out = jnp.concatenate([convolved_out[:, half:], convolved_out[:, :half]], axis=1)
+    mixed = (contract(retain_hidden, retain_full) + convolved_out).astype(jnp.bfloat16)
+    return swap_planes(lax.psum_scatter(mixed, "hi", scatter_dimension=0, tiled=True))
 
 
 def solution(mesh):
+    sp, tp = mesh.shape["sp"], mesh.shape["tp"]
+    planes = Mesh(mesh.devices.reshape(tp, sp // tp, tp), ("hi", "lo", "tp"))
     return jax.shard_map(
         local,
-        mesh=mesh,
+        mesh=planes,
         in_specs=(
-            P(("sp", "tp"), None),
-            P(),
-            P("sp", "tp"),
-            P("sp", "tp"),
-            P("sp", "tp"),
-            P("sp", "tp"),
-            P("sp", "tp"),
-            P("sp", "tp"),
-            P("sp", "tp"),
-            P(),
-            P(),
-            P(),
-            P("sp", "tp"),
-            P("sp", "tp"),
+            P(("hi", "lo", "tp"), None),
+            P(),
+            P(("hi", "lo"), "tp"),
+            P(("hi", "lo"), "tp"),
+            P(("hi", "lo"), "tp"),
+            P(("hi", "lo"), "tp"),
+            P(("hi", "lo"), "tp"),
+            P(("hi", "lo"), "tp"),
+            P(("hi", "lo"), "tp"),
+            P(),
+            P(),
+            P(),
+            P(("hi", "lo"), "tp"),
+            P(("hi", "lo"), "tp"),
         ),
-        out_specs=P(("sp", "tp"), None),
+        out_specs=P(("hi", "lo", "tp"), None),
         check_vma=False,
     )

time: 725 us -> 537 us (0.74)
  waiting for transfers between devices: 613 us -> 382 us
  starting transfers between devices: 2.89 us -> 48.7 us
  local copies, waits for them, and re-layouts: 8.88 us -> 30.5 us
  blocking collectives: 20.4 us -> 0 us
    all_gather x11 -> x10, waiting for transfers between devices: 579 us -> 109 us  [the longest x4 68 us: rolled(): return lax.all_gather(swap_planes_rolled(matrix), SPANS, axis=0, tiled=True)]
    ppermute x1 -> x16, waiting for transfers between devices: 0.01 us -> 230 us  [the longest x7 131 us: swap_planes(): return lax.ppermute(x, ('hi', 'tp'), pairs)]
    ppermute x1 -> x16, starting transfers between devices: 2.46 us -> 48.3 us  [the longest x7 32.7 us: swap_planes(): return lax.ppermute(x, ('hi', 'tp'), pairs)]
    all_gather x1 -> x0, blocking collectives: 20.4 us -> none  [carried_in(): gathered = jax.tree.map(lambda a: lax.all_gather(a, axis), part)]
    reduce_scatter x1, waiting for transfers between devices: 28.7 us -> 43.8 us  [local(): lax.psum_scatter(mixed, 'hi', scatter_dimension=0, tiled=True)]
    unnamed x18 -> x113, local copies, waits for them, and re-layouts: 0.8 us -> 13.5 us
    slice x1 -> x3, local copies, waits for them, and re-layouts: 0.01 us -> 8.17 us  [the longest x1 4.87 us: local(): convolved_out[:, half:]]
  transfers between devices with their start and end apart: 13 -> 27, of which waited for: 12 -> 20; matrix products, arithmetic and copies ran while one was open for 8% -> 13% of each run, Pallas kernels for 0% -> 0%
where the time goes in v1:
time: 537 us; the launch traced here: 536 us
  waiting for transfers between devices  382 us (71%)
  starting transfers between devices  48.7 us (9%)
  matrix products  43.7 us (8%)
  local copies, waits for them, and re-layouts  30.5 us (6%)
  other arithmetic  17 us (3%)
  between operations  14 us (3%)
    ppermute x7, waiting for transfers between devices, swap_planes(): return lax.ppermute(x, ('hi', 'tp'), pairs)  131 us
    all_gather x4, waiting for transfers between devices, rolled(): return lax.all_gather(swap_planes_rolled(matrix), SPANS, axis=0, tiled=True)  68 us
    ppermute x4, waiting for transfers between devices, swap_planes_rolled(): return lax.ppermute(x, ('hi', 'tp'), pairs)  63.3 us
    reduce_scatter x1, waiting for transfers between devices, local(): lax.psum_scatter(mixed, 'hi', scatter_dimension=0, tiled=True)  43.8 us
    all_gather x5, waiting for transfers between devices, straight(): return lax.all_gather(swap_planes(matrix), SPANS, axis=0, tiled=True)  40.7 us
    ppermute x5, waiting for transfers between devices, from_behind(): return lax.ppermute(x, ('lo', 'tp'), list(zip(spot[:-by], spot[by:])))  35.6 us
    ppermute x7, starting transfers between devices, swap_planes(): return lax.ppermute(x, ('hi', 'tp'), pairs)  32.7 us
    dot_general x2, matrix products, contract(): lax.dot_general(hidden, matrix, (((1,), (1,)), ((), ())), preferred_eleme...  19.3 us
  transfers between devices with their start and end apart: 27, of which 20 were waited for; matrix products, arithmetic and copies ran while one was open for 13% of the time, Pallas kernels for 0%

profile of v1, /device:TPU:2, one launch (start us, length us, event | category | flops | bytes accessed | tf_op | source)
XLA Modules:
  0.0 536.1 jit_solution(13960458750540282171)
XLA Ops:
  9.3 4.5 collective-permute-start
  13.7 27.7 %collective-permute-done = bf16[128,2048]{1,0:T(8,128)(2,1)S(1)} collective-permute-done((bf16[128,2048]{1,0:T(8,128)(2,1)S(1)}, bf16[128,2048]{1,0:T(8,128)(2,1)S(1)}, u32[]{:S(2)}, u32[]{:S(2)}) %collective-permute-start) | collective-permute-done | bytes 524320 | tf_op jit(solution)/shard_map/ppermute | solution.py:25
  44.2 33.9 %collective-permute-done.2 = bf16[256,512]{1,0:T(8,128)(2,1)S(1)} collective-permute-done((bf16[256,512]{1,0:T(8,128)(2,1)S(1)}, bf16[256,512]{1,0:T(8,128)(2,1)S(1)}, u32[]{:S(2)}, u32[]{:S(2)}) %collective-permute-start.2) | collective-permute-done | bytes 262176 | tf_op jit(solution)/shard_map/ppermute | solution.py:25
  80.9 22.9 %collective-permute-done.3 = bf16[256,512]{1,0:T(8,128)(2,1)S(1)} collective-permute-done((bf16[256,512]{1,0:T(8,128)(2,1)S(1)}, bf16[256,512]{1,0:T(8,128)(2,1)S(1)}, u32[]{:S(2)}, u32[]{:S(2)}) %collective-permute-start.3) | collective-permute-done | bytes 262176 | tf_op jit(solution)/shard_map/ppermute | solution.py:25
  104.6 6.4 %collective-permute-done.11 = bf16[256,512]{1,0:T(8,128)(2,1)S(1)} collective-permute-done((bf16[256,512]{1,0:T(8,128)(2,1)S(1)}, bf16[256,512]{1,0:T(8,128)(2,1)S(1)}, u32[]{:S(2)}, u32[]{:S(2)}) %collective-permute-start.11) | collective-permute-done | bytes 262176 | tf_op jit(solution)/shard_map/ppermute | solution.py:35
  111.7 5.1 collective-permute-start.10
  116.8 10.1 %collective-permute-done.10 = bf16[256,512]{1,0:T(8,128)(2,1)S(1)} collective-permute-done((bf16[256,512]{1,0:T(8,128)(2,1)}, bf16[256,512]{1,0:T(8,128)(2,1)S(1)}, u32[]{:S(2)}, u32[]{:S(2)}) %collective-permute-start.10) | collective-permute-done | bytes 262176 | tf_op jit(solution)/shard_map/ppermute | solution.py:25
  127.8 17.2 %collective-permute-done.1 = bf16[256,1024]{1,0:T(8,128)(2,1)S(1)} collective-permute-done((bf16[256,1024]{1,0:T(8,128)(2,1)S(1)}, bf16[256,1024]{1,0:T(8,128)(2,1)S(1)}, u32[]{:S(2)}, u32[]{:S(2)}) %collective-permute-start.1) | collective-permute-done | bytes 524320 | tf_op jit(solution)/shard_map/ppermute | solution.py:35
  145.8 12.4 %collective-permute-start.13 = (bf16[256,512]{1,0:T(8,128)(2,1)}, bf16[256,512]{1,0:T(8,128)(2,1)S(1)}, u32[]{:S(2)}, u32[]{:S(2)}) collective-permute-start(bf16[256,512]{1,0:T(8,128)(2,1)} %param.22), channel_id=1, source_target_pairs={{0,0},{1,8},{2,16},{3,24},{8,1},{9,9},{10,17},{11,25},{16,2},{17,1... | collective-permute-start | bytes 786440 | tf_op jit(solution)/shard_map/ppermute | solution.py:25
  158.2 8.6 %collective-permute-done.13 = bf16[256,512]{1,0:T(8,128)(2,1)S(1)} collective-permute-done((bf16[256,512]{1,0:T(8,128)(2,1)}, bf16[256,512]{1,0:T(8,128)(2,1)S(1)}, u32[]{:S(2)}, u32[]{:S(2)}) %collective-permute-start.13) | collective-permute-done | bytes 262176 | tf_op jit(solution)/shard_map/ppermute | solution.py:25
  167.7 12.0 %collective-permute-done.14 = bf16[256,512]{1,0:T(8,128)(2,1)S(1)} collective-permute-done((bf16[256,512]{1,0:T(8,128)(2,1)}, bf16[256,512]{1,0:T(8,128)(2,1)S(1)}, u32[]{:S(2)}, u32[]{:S(2)}) %collective-permute-start.14) | collective-permute-done | bytes 262176 | tf_op jit(solution)/shard_map/ppermute | solution.py:35
  182.0 27.8 %collective-permute-done.8 = bf16[256,1024]{1,0:T(8,128)(2,1)S(1)} collective-permute-done((bf16[256,1024]{1,0:T(8,128)(2,1)S(1)}, bf16[256,1024]{1,0:T(8,128)(2,1)S(1)}, u32[]{:S(2)}, u32[]{:S(2)}) %collective-permute-start.8) | collective-permute-done | bytes 524320 | tf_op jit(solution)/shard_map/ppermute | solution.py:35
  210.7 3.4 collective-permute-start.9
  230.2 3.3 fusion.104
  245.7 4.7 fusion.12
  259.7 31.3 %all-gather.13.cloned.1.call-done = bf16[2048,1024]{1,0:T(8,128)(2,1)} async-done(((bf16[256,1024]{1,0:T(8,128)(2,1)}), bf16[2048,1024]{1,0:T(8,128)(2,1)}) %all-gather.13.cloned.1.call-update) | async-done | bytes 4194320 | tf_op jit(solution)/shard_map/all_gather | solution.py:185
  291.1 4.5 convolution_convert_fusion.1
  299.2 4.7 fusion.102
  303.9 9.4 %collective-permute-done.4 = bf16[2,256,512]{2,1,0:T(8,128)(2,1)S(1)} collective-permute-done((bf16[2,256,512]{2,1,0:T(8,128)(2,1)S(1)}, bf16[2,256,512]{2,1,0:T(8,128)(2,1)S(1)}, u32[]{:S(2)}, u32[]{:S(2)}) %collective-permute-start.4) | collective-permute-done | bytes 524320 | tf_op jit(solution)/shard_map/ppermute | solution.py:41
  313.3 4.4 collective-permute-start.5
  317.9 16.7 %collective-permute-done.5 = bf16[2,256,512]{2,1,0:T(8,128)(2,1)S(1)} collective-permute-done((bf16[2,256,512]{2,1,0:T(8,128)(2,1)S(1)}, bf16[2,256,512]{2,1,0:T(8,128)(2,1)S(1)}, u32[]{:S(2)}, u32[]{:S(2)}) %collective-permute-start.5) | collective-permute-done | bytes 524320 | tf_op jit(solution)/shard_map/ppermute | solution.py:41
  338.0 27.0 %all-gather.29.cloned.1.call-done = bf16[2048,512]{1,0:T(8,128)(2,1)} async-done(((bf16[256,512]{1,0:T(8,128)(2,1)}), bf16[2048,512]{1,0:T(8,128)(2,1)}) %all-gather.29.cloned.1.call-update) | async-done | bytes 2097168 | tf_op jit(solution)/shard_map/all_gather | solution.py:185
  365.0 7.6 %fusion.27 = f32[512,2048]{1,0:T(8,128)} fusion(bf16[2048,512]{1,0:T(8,128)(2,1)} %all-gather.29.cloned.1.call-done, bf16[512,2048]{1,0:T(8,128)(2,1)} %all-gather.11.cloned.1.call-done, bf16[2048,512]{1,0:T(8,128)(2,1)} %all-gather.27.cloned.1.call-done, f32[512,512]{1,0:T(8,128)S(1)} %get-tuple-element.6, f32[512]{0:T(512)S(1)} %copy-done.42, ...), kind=kOutput, calls=%fused_computation.77 | convolution fusion | flops 2151677952 | bytes 11542528 | tf_op jit(solution)/shard_map/dot_general | solution.py:150
  375.2 4.9 fusion.103
  380.1 3.3 fusion.7
  383.4 9.5 %collective-permute-done.7 = bf16[2,256,512]{2,1,0:T(8,128)(2,1)} collective-permute-done((bf16[2,256,512]{2,1,0:T(8,128)(2,1)}, bf16[2,256,512]{2,1,0:T(8,128)(2,1)}, u32[]{:S(2)}, u32[]{:S(2)}) %collective-permute-start.7) | collective-permute-done | bytes 524320 | tf_op jit(solution)/shard_map/ppermute | solution.py:41
  397.5 9.6 %all-gather.19.cloned.1.call-done = bf16[2048,1024]{1,0:T(8,128)(2,1)} async-done(((bf16[256,1024]{1,0:T(8,128)(2,1)}), bf16[2048,1024]{1,0:T(8,128)(2,1)}) %all-gather.19.cloned.1.call-update) | async-done | bytes 4194320 | tf_op jit(solution)/shard_map/all_gather | solution.py:185
  407.1 38.3 %all-gather.21.cloned.1.call-done = bf16[2048,1024]{1,0:T(8,128)(2,1)} async-done(((bf16[256,1024]{1,0:T(8,128)(2,1)}), bf16[2048,1024]{1,0:T(8,128)(2,1)}) %all-gather.21.cloned.1.call-update) | async-done | bytes 4194320 | tf_op jit(solution)/shard_map/all_gather | solution.py:182
  445.5 11.7 %fusion = bf16[512,2048]{1,0:T(8,128)(2,1)} fusion(f32[512,1024]{1,0:T(8,128)} %get-tuple-element.8, f32[512,1024]{1,0:T(8,128)} %get-tuple-element.7, bf16[2048,1024]{1,0:T(8,128)(2,1)} %all-gather.21.cloned.1.call-done, f32[512,1024]{1,0:T(8,128)} %copy.23, bf16[2048,1024]{1,0:T(8,128)(2,1)} %all-gather.19.cloned.1.call-done, ...), kind=kOutput, calls=%fused_computation.30 | convolution fusion | flops 4306501632 | bytes 18874368 | tf_op jit(solution)/shard_map/dot_general | solution.py:150
  457.2 43.8 %reduce-scatter.2.cloned.1.call-done = bf16[128,2048]{1,0:T(8,128)(2,1)} async-done(((bf16[512,2048]{1,0:T(8,128)(2,1)}), bf16[128,2048]{1,0:T(8,128)(2,1)}) %reduce-scatter.2.cloned.1.call-update) | async-done | bytes 524304 | tf_op jit(solution)/shard_map/reduce_scatter | solution.py:224
  501.0 3.5 collective-permute-start.15
  504.5 24.3 %collective-permute-done.15 = bf16[128,2048]{1,0:T(8,128)(2,1)S(1)} collective-permute-done((bf16[128,2048]{1,0:T(8,128)(2,1)}, bf16[128,2048]{1,0:T(8,128)(2,1)S(1)}, u32[]{:S(2)}, u32[]{:S(2)}) %collective-permute-start.15) | collective-permute-done | bytes 524320 | tf_op jit(solution)/shard_map/ppermute | solution.py:25
  (191 shorter events, 67.7 us)
Async XLA Ops:
  6.5 72.4 %copy-start.51 = (bf16[256,512]{1,0:T(8,128)(2,1)S(1)}, bf16[256,512]{1,0:T(8,128)(2,1)}, u32[]{:S(2)}) copy-start(bf16[256,512]{1,0:T(8,128)(2,1)} %param.17) | copy-start | bytes 786436
  6.5 98.0 %copy-start.52 = (bf16[256,512]{1,0:T(8,128)(2,1)S(1)}, bf16[256,512]{1,0:T(8,128)(2,1)}, u32[]{:S(2)}) copy-start(bf16[256,512]{1,0:T(8,128)(2,1)} %param.21) | copy-start | bytes 786436
  6.5 121.1 %copy-start.47 = (bf16[256,1024]{1,0:T(8,128)(2,1)S(1)}, bf16[256,1024]{1,0:T(8,128)(2,1)}, u32[]{:S(2)}) copy-start(bf16[256,1024]{1,0:T(8,128)(2,1)} %param.18) | copy-start | bytes 1572868
  6.5 174.0 %copy-start.48 = (bf16[256,1024]{1,0:T(8,128)(2,1)S(1)}, bf16[256,1024]{1,0:T(8,128)(2,1)}, u32[]{:S(2)}) copy-start(bf16[256,1024]{1,0:T(8,128)(2,1)} %param.19) | copy-start | bytes 1572868
  6.5 223.6 %all-gather.11.cloned.1.call-start = ((), (), s32[]{:S(2)}) async-start(), calls=%async_computation.1 | async-start | bytes 2621440 | tf_op jit(solution)/shard_map/all_gather | solution.py:175
  8.0 202.7 %copy-start.49 = (bf16[256,1024]{1,0:T(8,128)(2,1)S(1)}, bf16[256,1024]{1,0:T(8,128)(2,1)}, u32[]{:S(2)}) copy-start(bf16[256,1024]{1,0:T(8,128)(2,1)} %param.26) | copy-start | bytes 1572868
  9.3 32.2 %collective-permute-start = (bf16[128,2048]{1,0:T(8,128)(2,1)S(1)}, bf16[128,2048]{1,0:T(8,128)(2,1)S(1)}, u32[]{:S(2)}, u32[]{:S(2)}) collective-permute-start(bf16[128,2048]{1,0:T(8,128)(2,1)S(1)} %fusion.18), channel_id=1, source_target_pairs={{0,0},{1,8},{2,16},{3,24},{8,1},{9,9},{10,17},{11,25},{16,2},{17,1... | collective-permute-start | bytes 1572872 | tf_op jit(solution)/shard_map/ppermute | solution.py:25
  42.3 191.2 %all-gather.15.cloned.1.call-start = ((), (), s32[]{:S(2)}) async-start(), calls=%async_computation.3 | async-start | bytes 2359296 | tf_op jit(solution)/shard_map/all_gather | solution.py:182
  42.3 35.8 %collective-permute-start.2 = (bf16[256,512]{1,0:T(8,128)(2,1)S(1)}, bf16[256,512]{1,0:T(8,128)(2,1)S(1)}, u32[]{:S(2)}, u32[]{:S(2)}) collective-permute-start(bf16[256,512]{1,0:T(8,128)(2,1)S(1)} %copy-done.50), channel_id=1, source_target_pairs={{0,0},{1,8},{2,16},{3,24},{8,1},{9,9},{10,17},{11,25},{16,2},{17,1... | collective-permute-start | bytes 786440 | tf_op jit(solution)/shard_map/ppermute | solution.py:25
  78.9 157.7 %all-gather.17.cloned.1.call-start = ((), (), s32[]{:S(2)}) async-start(), calls=%async_computation.4 | async-start | bytes 2359296 | tf_op jit(solution)/shard_map/all_gather | solution.py:182
  78.9 24.8 %collective-permute-start.3 = (bf16[256,512]{1,0:T(8,128)(2,1)S(1)}, bf16[256,512]{1,0:T(8,128)(2,1)S(1)}, u32[]{:S(2)}, u32[]{:S(2)}) collective-permute-start(bf16[256,512]{1,0:T(8,128)(2,1)S(1)} %copy-done.51), channel_id=1, source_target_pairs={{0,0},{1,8},{2,16},{3,24},{8,1},{9,9},{10,17},{11,25},{16,2},{17,1... | collective-permute-start | bytes 786440 | tf_op jit(solution)/shard_map/ppermute | solution.py:25
  104.5 141.2 %all-gather.25.cloned.1.call-start = ((), (), s32[]{:S(2)}) async-start(), calls=%async_computation.8 | async-start | bytes 2359296 | tf_op jit(solution)/shard_map/all_gather | solution.py:185
  104.5 6.4 %collective-permute-start.11 = (bf16[256,512]{1,0:T(8,128)(2,1)S(1)}, bf16[256,512]{1,0:T(8,128)(2,1)S(1)}, u32[]{:S(2)}, u32[]{:S(2)}) collective-permute-start(bf16[256,512]{1,0:T(8,128)(2,1)S(1)} %copy-done.52), channel_id=1, source_target_pairs={{0,2},{1,10},{2,18},{3,26},{8,3},{9,11},{10,19},{11,27},{16,0},{17... | collective-permute-start | bytes 786440 | tf_op jit(solution)/shard_map/ppermute | solution.py:35
  111.7 141.0 %all-gather.23.cloned.1.call-start = ((), (), s32[]{:S(2)}) async-start(), calls=%async_computation.7 | async-start | bytes 2359296 | tf_op jit(solution)/shard_map/all_gather | solution.py:182
  111.7 15.2 %collective-permute-start.10 = (bf16[256,512]{1,0:T(8,128)(2,1)}, bf16[256,512]{1,0:T(8,128)(2,1)S(1)}, u32[]{:S(2)}, u32[]{:S(2)}) collective-permute-start(bf16[256,512]{1,0:T(8,128)(2,1)} %param.20), channel_id=1, source_target_pairs={{0,0},{1,8},{2,16},{3,24},{8,1},{9,9},{10,17},{11,25},{16,2},{17,1... | collective-permute-start | bytes 786440 | tf_op jit(solution)/shard_map/ppermute | solution.py:25
  127.6 163.4 %all-gather.13.cloned.1.call-start = ((), (), s32[]{:S(2)}) async-start(), calls=%async_computation.2 | async-start | bytes 4718592 | tf_op jit(solution)/shard_map/all_gather | solution.py:185
  127.7 17.3 %collective-permute-start.1 = (bf16[256,1024]{1,0:T(8,128)(2,1)S(1)}, bf16[256,1024]{1,0:T(8,128)(2,1)S(1)}, u32[]{:S(2)}, u32[]{:S(2)}) collective-permute-start(bf16[256,1024]{1,0:T(8,128)(2,1)S(1)} %copy-done.47), channel_id=1, source_target_pairs={{0,2},{1,10},{2,18},{3,26},{8,3},{9,11},{10,19},{11,27},{16,0},{17... | collective-permute-start | bytes 1572872 | tf_op jit(solution)/shard_map/ppermute | solution.py:35
  145.8 192.2 %all-gather.27.cloned.1.call-start = ((), (), s32[]{:S(2)}) async-start(), calls=%async_computation.9 | async-start | bytes 2359296 | tf_op jit(solution)/shard_map/all_gather | solution.py:182
  145.8 21.0 %collective-permute-start.13 = (bf16[256,512]{1,0:T(8,128)(2,1)}, bf16[256,512]{1,0:T(8,128)(2,1)S(1)}, u32[]{:S(2)}, u32[]{:S(2)}) collective-permute-start(bf16[256,512]{1,0:T(8,128)(2,1)} %param.22), channel_id=1, source_target_pairs={{0,0},{1,8},{2,16},{3,24},{8,1},{9,9},{10,17},{11,25},{16,2},{17,1... | collective-permute-start | bytes 786440 | tf_op jit(solution)/shard_map/ppermute | solution.py:25
  167.6 197.4 %all-gather.29.cloned.1.call-start = ((), (), s32[]{:S(2)}) async-start(), calls=%async_computation.10 | async-start | bytes 2359296 | tf_op jit(solution)/shard_map/all_gather | solution.py:185
  167.7 12.1 %collective-permute-start.14 = (bf16[256,512]{1,0:T(8,128)(2,1)}, bf16[256,512]{1,0:T(8,128)(2,1)S(1)}, u32[]{:S(2)}, u32[]{:S(2)}) collective-permute-start(bf16[256,512]{1,0:T(8,128)(2,1)} %param.27), channel_id=1, source_target_pairs={{0,2},{1,10},{2,18},{3,26},{8,3},{9,11},{10,19},{11,27},{16,0},{17... | collective-permute-start | bytes 786440 | tf_op jit(solution)/shard_map/ppermute | solution.py:35
  180.5 226.7 %all-gather.19.cloned.1.call-start = ((), (), s32[]{:S(2)}) async-start(), calls=%async_computation.5 | async-start | bytes 4718592 | tf_op jit(solution)/shard_map/all_gather | solution.py:185
  180.5 29.3 %collective-permute-start.8 = (bf16[256,1024]{1,0:T(8,128)(2,1)S(1)}, bf16[256,1024]{1,0:T(8,128)(2,1)S(1)}, u32[]{:S(2)}, u32[]{:S(2)}) collective-permute-start(bf16[256,1024]{1,0:T(8,128)(2,1)S(1)} %copy-done.48), channel_id=1, source_target_pairs={{0,2},{1,10},{2,18},{3,26},{8,3},{9,11},{10,19},{11,27},{16,0},{17... | collective-permute-start | bytes 1572872 | tf_op jit(solution)/shard_map/ppermute | solution.py:35
  210.6 234.8 %all-gather.21.cloned.1.call-start = ((), (), s32[]{:S(2)}) async-start(), calls=%async_computation.6 | async-start | bytes 4718592 | tf_op jit(solution)/shard_map/all_gather | solution.py:182
  210.7 18.6 %collective-permute-start.9 = (bf16[256,1024]{1,0:T(8,128)(2,1)S(1)}, bf16[256,1024]{1,0:T(8,128)(2,1)S(1)}, u32[]{:S(2)}, u32[]{:S(2)}) collective-permute-start(bf16[256,1024]{1,0:T(8,128)(2,1)S(1)} %copy-done.49), channel_id=1, source_target_pairs={{0,0},{1,8},{2,16},{3,24},{8,1},{9,9},{10,17},{11,25},{16,2},{17,1... | collective-permute-start | bytes 1572872 | tf_op jit(solution)/shard_map/ppermute | solution.py:25
  230.1 270.9 %reduce-scatter.2.cloned.1.call-start = ((), (), s32[]{:S(2)}) async-start(), calls=%async_computation.11 | async-start | bytes 2621440 | tf_op jit(solution)/shard_map/reduce_scatter | solution.py:224
  256.0 43.1 %collective-permute-start.12 = (bf16[30,512]{1,0:T(8,128)(2,1)S(1)}, bf16[30,512]{1,0:T(8,128)(2,1)S(1)}, u32[]{:S(2)}, u32[]{:S(2)}) collective-permute-start(bf16[30,512]{1,0:T(8,128)(2,1)S(1)} %slice.286), channel_id=1, source_target_pairs={{0,4},{4,1},{1,5},{5,2},{2,6},{6,3},{3,7},{8,12},{12,9},{9,13},{13... | collective-permute-start | bytes 92168 | tf_op jit(solution)/shard_map/ppermute | solution.py:41
  296.4 16.9 %collective-permute-start.4 = (bf16[2,256,512]{2,1,0:T(8,128)(2,1)S(1)}, bf16[2,256,512]{2,1,0:T(8,128)(2,1)S(1)}, u32[]{:S(2)}, u32[]{:S(2)}) collective-permute-start(bf16[2,256,512]{2,1,0:T(8,128)(2,1)S(1)} %convolution_convert_fusion.7), channel_id=1, source_target_pairs={{0,4},{4,1},{1,5},{5,2},{2,6},{6,3},{3,7},{8,12},{12,9},{9,13},{13... | collective-permute-start | bytes 1572872 | tf_op jit(solution)/shard_map/ppermute | solution.py:41
  313.3 21.4 %collective-permute-start.5 = (bf16[2,256,512]{2,1,0:T(8,128)(2,1)S(1)}, bf16[2,256,512]{2,1,0:T(8,128)(2,1)S(1)}, u32[]{:S(2)}, u32[]{:S(2)}) collective-permute-start(bf16[2,256,512]{2,1,0:T(8,128)(2,1)S(1)} %collective-permute-done.4), channel_id=1, source_target_pairs={{0,4},{4,1},{1,5},{5,2},{2,6},{6,3},{3,7},{8,12},{12,9},{9,13},{13... | collective-permute-start | bytes 1572872 | tf_op jit(solution)/shard_map/ppermute | solution.py:41
  335.0 37.7 %collective-permute-start.6 = (bf16[2,256,512]{2,1,0:T(8,128)(2,1)S(1)}, bf16[2,256,512]{2,1,0:T(8,128)(2,1)S(1)}, u32[]{:S(2)}, u32[]{:S(2)}) collective-permute-start(bf16[2,256,512]{2,1,0:T(8,128)(2,1)S(1)} %fusion.41), channel_id=1, source_target_pairs={{0,1},{4,5},{1,2},{5,6},{2,3},{6,7},{8,9},{12,13},{9,10},{13,14},{... | collective-permute-start | bytes 1572872 | tf_op jit(solution)/shard_map/ppermute | solution.py:41
  373.8 19.1 %collective-permute-start.7 = (bf16[2,256,512]{2,1,0:T(8,128)(2,1)}, bf16[2,256,512]{2,1,0:T(8,128)(2,1)}, u32[]{:S(2)}, u32[]{:S(2)}) collective-permute-start(bf16[2,256,512]{2,1,0:T(8,128)(2,1)} %fusion.44), channel_id=1, source_target_pairs={{0,2},{4,6},{1,3},{5,7},{8,10},{12,14},{9,11},{13,15},{16,18},{20,... | collective-permute-start | bytes 1572872 | tf_op jit(solution)/shard_map/ppermute | solution.py:41
  501.0 27.8 %collective-permute-start.15 = (bf16[128,2048]{1,0:T(8,128)(2,1)}, bf16[128,2048]{1,0:T(8,128)(2,1)S(1)}, u32[]{:S(2)}, u32[]{:S(2)}) collective-permute-start(bf16[128,2048]{1,0:T(8,128)(2,1)} %reduce-scatter.2.cloned.1.call-done), channel_id=1, source_target_pairs={{0,0},{1,8},{2,16},{3,24},{8,1},{9,9},{10,17},{11,25},{16,2},{17,1... | collective-permute-start | bytes 1572872 | tf_op jit(solution)/shard_map/ppermute | solution.py:25
  (49 other events, 621.8 us)
Sparse Core Ops, SparseCore 0:
  42.4 51.0 all-gather.10
  95.4 48.8 all-gather.14
  146.2 34.9 all-gather.16
  183.0 34.6 all-gather.24
  219.4 33.2 all-gather.22
  254.4 36.5 all-gather.12
  292.9 41.5 all-gather.26
  336.4 28.5 all-gather.28
  366.9 40.1 all-gather.18
  408.8 36.5 all-gather.20
  457.3 43.6 reduce-scatter.1

commit v2 on v1

--- a/solution.py
+++ b/solution.py
@@ -178,24 +178,24 @@
     half = normed.shape[1] // 2
     normed_rolled = jnp.concatenate([normed[:, half:], normed[:, :half]], axis=1)
 
-    def straight(matrix):
-        return lax.all_gather(swap_planes(matrix), SPANS, axis=0, tiled=True)
-
-    def rolled(matrix):
-        return lax.all_gather(swap_planes_rolled(matrix), SPANS, axis=0, tiled=True)
-
-    def project(rows, matrix):
-        return jnp.dot(rows, matrix, preferred_element_type=jnp.float32).astype(jnp.bfloat16)
-
-    key_rows = project(normed, straight(key_weight))
-    values = project(normed_rolled, rolled(value_weight))
-    queries = project(normed, straight(query_weight))
-    glu_value = project(normed, straight(unit_value))
-    glu_switch = project(normed_rolled, rolled(unit_gate))
-    convolve_switch = project(normed, straight(convolve_gate))
-    retain_switch = project(normed_rolled, rolled(retain_gate))
-    convolve_full = rolled(convolve_output)
-    retain_full = straight(retain_output)
+    def gathered(swap, *matrices):
+        return lax.all_gather(
+            swap(jnp.concatenate(matrices, axis=1)), SPANS, axis=0, tiled=True
+        )
+
+    def project(rows, merged, *matrices):
+        product = jnp.dot(rows, merged, preferred_element_type=jnp.float32).astype(jnp.bfloat16)
+        ends = [sum(m.shape[1] for m in matrices[: k + 1]) for k in range(len(matrices) - 1)]
+        return jnp.split(product, ends, axis=1)
+
+    first = (key_weight, value_weight, query_weight)
+    second = (unit_value, unit_gate, convolve_gate, retain_gate)
+    third = (retain_output, convolve_output)
+    key_rows, values, queries = project(normed, gathered(swap_planes, *first), *first)
+    glu_value, glu_switch, convolve_switch, retain_switch = project(
+        normed_rolled, gathered(swap_planes_rolled, *second), *second
+    )
+    out_full = gathered(swap_planes, *third)
     row_count = normed.shape[0]
     local_heads = queries.shape[1] // KEY
     positions = chain_rank * row_count + jnp.arange(row_count, dtype=jnp.int32)
@@ -218,9 +218,8 @@
     convolve_hidden = convolve_branch(
         gated_input, before, tap_slice, gain_slice, shift_slice, convolve_switch
     )
-    convolved_out = contract(convolve_hidden, convolve_full)
-    convolved_out = jnp.concatenate([convolved_out[:, half:], convolved_out[:, :half]], axis=1)
-    mixed = (contract(retain_hidden, retain_full) + convolved_out).astype(jnp.bfloat16)
+    hidden = jnp.concatenate([retain_hidden, convolve_hidden], axis=1)
+    mixed = contract(hidden, out_full).astype(jnp.bfloat16)
     return swap_planes(lax.psum_scatter(mixed, "hi", scatter_dimension=0, tiled=True))
 
 

time: 537 us -> 447 us (0.83)
  waiting for transfers between devices: 382 us -> 316 us
  local copies, waits for them, and re-layouts: 30.5 us -> 16.6 us
  matrix products: 43.7 us -> 30.8 us
    all_gather x9 -> x3, waiting for transfers between devices: 109 us -> 13.4 us  [gathered(): lax.all_gather(swap(jnp.concatenate(matrices, axis=1)), SPANS, axis=0, ti...]
    ppermute x7 -> x4, waiting for transfers between devices: 131 us -> 177 us  [swap_planes(): return lax.ppermute(x, ('hi', 'tp'), pairs)]
    ppermute x4 -> x1, waiting for transfers between devices: 63.3 us -> 28.8 us  [swap_planes_rolled(): return lax.ppermute(x, ('hi', 'tp'), pairs)]
    ppermute x5, waiting for transfers between devices: 35.6 us -> 52.8 us  [from_behind(): return lax.ppermute(x, ('lo', 'tp'), list(zip(spot[:-by], spot[by:])))]
    dot_general x2 -> x1, matrix products: 19.3 us -> 7.41 us  [contract(): lax.dot_general(hidden, matrix, (((1,), (1,)), ((), ())), preferred_eleme...]
    unnamed x113 -> x39, local copies, waits for them, and re-layouts: 13.5 us -> 5.63 us
    ppermute x5, starting transfers between devices: 13.9 us -> 21.5 us  [from_behind(): return lax.ppermute(x, ('lo', 'tp'), list(zip(spot[:-by], spot[by:])))]
    ppermute x7 -> x4, starting transfers between devices: 32.7 us -> 25.5 us  [swap_planes(): return lax.ppermute(x, ('hi', 'tp'), pairs)]
  transfers between devices with their start and end apart: 27 -> 15, of which waited for: 20 -> 12; matrix products, arithmetic and copies ran while one was open for 13% -> 12% of each run, Pallas kernels for 0% -> 0%
where the time goes in v2:
time: 447 us; the launch traced here: 446 us
  waiting for transfers between devices  316 us (71%)
  starting transfers between devices  47.2 us (11%)
  matrix products  30.8 us (7%)
  other arithmetic  21.4 us (5%)
  local copies, waits for them, and re-layouts  16.6 us (4%)
  between operations  13.6 us (3%)
    ppermute x4, waiting for transfers between devices, swap_planes(): return lax.ppermute(x, ('hi', 'tp'), pairs)  177 us
    ppermute x5, waiting for transfers between devices, from_behind(): return lax.ppermute(x, ('lo', 'tp'), list(zip(spot[:-by], spot[by:])))  52.8 us
    reduce_scatter x1, waiting for transfers between devices, local(): lax.psum_scatter(mixed, 'hi', scatter_dimension=0, tiled=True)  43.8 us
    ppermute x1, waiting for transfers between devices, swap_planes_rolled(): return lax.ppermute(x, ('hi', 'tp'), pairs)  28.8 us
    ppermute x4, starting transfers between devices, swap_planes(): return lax.ppermute(x, ('hi', 'tp'), pairs)  25.5 us
    ppermute x5, starting transfers between devices, from_behind(): return lax.ppermute(x, ('lo', 'tp'), list(zip(spot[:-by], spot[by:])))  21.5 us
    dot_general x2, matrix products, project(): jnp.dot(rows, merged, preferred_element_type=jnp.float32)  17.3 us
    all_gather x3, waiting for transfers between devices, gathered(): lax.all_gather(swap(jnp.concatenate(matrices, axis=1)), SPANS, axis=0, ti...  13.4 us
  transfers between devices with their start and end apart: 15, of which 12 were waited for; matrix products, arithmetic and copies ran while one was open for 12% of the time, Pallas kernels for 0%

profile of v2, /device:TPU:2, one launch (start us, length us, event | category | flops | bytes accessed | tf_op | source)
XLA Modules:
  0.0 446.0 jit_solution(2399027027549937023)
XLA Ops:
  6.5 1.3 fusion.13
  9.1 4.6 %collective-permute-start = (bf16[128,2048]{1,0:T(8,128)(2,1)S(1)}, bf16[128,2048]{1,0:T(8,128)(2,1)S(1)}, u32[]{:S(2)}, u32[]{:S(2)}) collective-permute-start(bf16[128,2048]{1,0:T(8,128)(2,1)S(1)} %fusion.15), channel_id=1, source_target_pairs={{0,0},{1,8},{2,16},{3,24},{8,1},{9,9},{10,17},{11,25},{16,2},{17,1... | collective-permute-start | bytes 1572872 | tf_op jit(solution)/shard_map/ppermute | solution.py:25
  13.8 36.0 %collective-permute-done = bf16[128,2048]{1,0:T(8,128)(2,1)S(1)} collective-permute-done((bf16[128,2048]{1,0:T(8,128)(2,1)S(1)}, bf16[128,2048]{1,0:T(8,128)(2,1)S(1)}, u32[]{:S(2)}, u32[]{:S(2)}) %collective-permute-start) | collective-permute-done | bytes 524320 | tf_op jit(solution)/shard_map/ppermute | solution.py:25
  50.8 1.9 collective-permute-start.1
  52.7 93.0 %collective-permute-done.1 = bf16[256,2048]{1,0:T(8,128)(2,1)S(1)} collective-permute-done((bf16[256,2048]{1,0:T(8,128)(2,1)S(1)}, bf16[256,2048]{1,0:T(8,128)(2,1)S(1)}, u32[]{:S(2)}, u32[]{:S(2)}) %collective-permute-start.1) | collective-permute-done | bytes 1048608 | tf_op jit(solution)/shard_map/ppermute | solution.py:25
  148.0 28.8 %collective-permute-done.6 = bf16[256,2560]{1,0:T(8,128)(2,1)S(1)} collective-permute-done((bf16[256,2560]{1,0:T(8,128)(2,1)S(1)}, bf16[256,2560]{1,0:T(8,128)(2,1)S(1)}, u32[]{:S(2)}, u32[]{:S(2)}) %collective-permute-start.6) | collective-permute-done | bytes 1310752 | tf_op jit(solution)/shard_map/ppermute | solution.py:35
  178.1 15.5 %collective-permute-start.8 = (bf16[256,1536]{1,0:T(8,128)(2,1)S(1)}, bf16[256,1536]{1,0:T(8,128)(2,1)S(1)}, u32[]{:S(2)}, u32[]{:S(2)}) collective-permute-start(bf16[256,1536]{1,0:T(8,128)(2,1)S(1)} %pad_maximum_fusion.2), channel_id=1, source_target_pairs={{0,0},{1,8},{2,16},{3,24},{8,1},{9,9},{10,17},{11,25},{16,2},{17,1... | collective-permute-start | bytes 2359304 | tf_op jit(solution)/shard_map/ppermute | solution.py:25
  193.6 1.8 multiply_cosine_fusion
  195.4 24.1 %collective-permute-done.8 = bf16[256,1536]{1,0:T(8,128)(2,1)S(1)} collective-permute-done((bf16[256,1536]{1,0:T(8,128)(2,1)S(1)}, bf16[256,1536]{1,0:T(8,128)(2,1)S(1)}, u32[]{:S(2)}, u32[]{:S(2)}) %collective-permute-start.8) | collective-permute-done | bytes 786464 | tf_op jit(solution)/shard_map/ppermute | solution.py:25
  220.6 8.5 %convolution_convert_fusion.2 = bf16[512,2048]{1,0:T(8,128)(2,1)S(1)} fusion(bf16[512,2048]{1,0:T(8,128)(2,1)} %all-gather.5.cloned.1.call-done, bf16[2048,2048]{1,0:T(8,128)(2,1)} %all-gather.7.cloned.1.call-done), kind=kOutput, calls=%fused_computation.31 | convolution fusion | flops 4296015872 | bytes 12582912 | tf_op jit(solution)/shard_map/dot_general | solution.py:187
  235.3 3.4 collective-permute-start.2
  238.7 21.2 %collective-permute-done.2 = bf16[2,256,512]{2,1,0:T(8,128)(2,1)S(1)} collective-permute-done((bf16[2,256,512]{2,1,0:T(8,128)(2,1)S(1)}, bf16[2,256,512]{2,1,0:T(8,128)(2,1)S(1)}, u32[]{:S(2)}, u32[]{:S(2)}) %collective-permute-start.2) | collective-permute-done | bytes 524320 | tf_op jit(solution)/shard_map/ppermute | solution.py:41
  260.0 4.4 collective-permute-start.3
  264.4 14.3 %collective-permute-done.3 = bf16[2,256,512]{2,1,0:T(8,128)(2,1)S(1)} collective-permute-done((bf16[2,256,512]{2,1,0:T(8,128)(2,1)S(1)}, bf16[2,256,512]{2,1,0:T(8,128)(2,1)S(1)}, u32[]{:S(2)}, u32[]{:S(2)}) %collective-permute-start.3) | collective-permute-done | bytes 524320 | tf_op jit(solution)/shard_map/ppermute | solution.py:41
  279.8 6.6 %collective-permute-start.4 = (bf16[2,256,512]{2,1,0:T(8,128)(2,1)}, bf16[2,256,512]{2,1,0:T(8,128)(2,1)}, u32[]{:S(2)}, u32[]{:S(2)}) collective-permute-start(bf16[2,256,512]{2,1,0:T(8,128)(2,1)} %fusion.30), channel_id=1, source_target_pairs={{0,1},{4,5},{1,2},{5,6},{2,3},{6,7},{8,9},{12,13},{9,10},{13,14},{... | collective-permute-start | bytes 1572872 | tf_op jit(solution)/shard_map/ppermute | solution.py:41
  293.2 8.9 %collective-permute-done.4 = bf16[2,256,512]{2,1,0:T(8,128)(2,1)} collective-permute-done((bf16[2,256,512]{2,1,0:T(8,128)(2,1)}, bf16[2,256,512]{2,1,0:T(8,128)(2,1)}, u32[]{:S(2)}, u32[]{:S(2)}) %collective-permute-start.4) | collective-permute-done | bytes 524320 | tf_op jit(solution)/shard_map/ppermute | solution.py:41
  302.1 2.2 fusion.33
  304.3 1.5 collective-permute-start.5
  305.8 1.6 fusion.83
  307.4 3.3 fusion.12
  310.7 7.1 %collective-permute-done.5 = bf16[2,256,512]{2,1,0:T(8,128)(2,1)} collective-permute-done((bf16[2,256,512]{2,1,0:T(8,128)(2,1)}, bf16[2,256,512]{2,1,0:T(8,128)(2,1)}, u32[]{:S(2)}, u32[]{:S(2)}) %collective-permute-start.5) | collective-permute-done | bytes 524320 | tf_op jit(solution)/shard_map/ppermute | solution.py:41
  317.8 2.2 fusion.87
  320.2 1.6 subtract_multiply_fusion
  321.9 2.2 copy.23
  324.1 8.8 %convolution_convert_fusion = bf16[512,2560]{1,0:T(8,128)(2,1)S(1)} fusion(bf16[2048,2560]{1,0:T(8,128)(2,1)} %all-gather.9.cloned.1.call-done, bf16[512,1024]{1,0:T(8,128)(2,1)} %get-tuple-element.10, bf16[512,1024]{1,0:T(8,128)(2,1)S(1)} %copy-done.5), kind=kOutput, calls=%fused_computation.29 | convolution fusion | flops 5374214144 | bytes 15204352 | tf_op jit(solution)/shard_map/dot_general | solution.py:187
  333.3 5.6 %collective-permute-start.7 = (bf16[30,512]{1,0:T(8,128)(2,1)S(1)}, bf16[30,512]{1,0:T(8,128)(2,1)S(1)}, u32[]{:S(2)}, u32[]{:S(2)}) collective-permute-start(bf16[30,512]{1,0:T(8,128)(2,1)S(1)} %slice.278), channel_id=1, source_target_pairs={{0,4},{4,1},{1,5},{5,2},{2,6},{6,3},{3,7},{8,12},{12,9},{9,13},{13... | collective-permute-start | bytes 92168 | tf_op jit(solution)/shard_map/ppermute | solution.py:41
  340.8 4.6 %fusion.82 = (f32[512]{0:T(512)S(1)}, f32[512,512]{1,0:T(8,128)S(1)}) fusion(f32[512]{0:T(512)S(1)} %bitcast.63, bf16[512,512]{1,0:T(8,128)(2,1)S(1)} %multiply_convert_fusion.1, f32[512]{0:T(512)S(1)} %bitcast.65, bf16[30,512]{1,0:T(8,128)(2,1)S(1)} %collective-permute-done.7, f32[512]{0:T(512)S(1)} %bitcast.66, f32[512]{0:T(512)S(1)} %bitcast.67, ...), kind=kLoop, calls=%fused_computation.163 | loop fusion | flops 47971840 | bytes 1669120 | tf_op jit(solution)/shard_map/reduce_sum | solution.py:142
  346.3 13.4 %all-gather.11.cloned.1.call-done = bf16[2048,1536]{1,0:T(8,128)(2,1)} async-done(((bf16[256,1536]{1,0:T(8,128)(2,1)}), bf16[2048,1536]{1,0:T(8,128)(2,1)}) %all-gather.11.cloned.1.call-update) | async-done | bytes 6291472 | tf_op jit(solution)/shard_map/all_gather | solution.py:182
  359.7 7.4 %convolution_convert_fusion.1 = bf16[512,2048]{1,0:T(8,128)(2,1)} fusion(bf16[2048,1536]{1,0:T(8,128)(2,1)} %all-gather.11.cloned.1.call-done, bf16[512,512]{1,0:T(8,128)(2,1)S(1)} %fusion.28, bf16[512,1024]{1,0:T(8,128)(2,1)S(1)} %fusion.8), kind=kOutput, calls=%fused_computation.30 | convolution fusion | flops 3225419776 | bytes 9961472 | tf_op jit(solution)/shard_map/dot_general | solution.py:150
  367.1 43.8 %reduce-scatter.2.cloned.1.call-done = bf16[128,2048]{1,0:T(8,128)(2,1)} async-done(((bf16[512,2048]{1,0:T(8,128)(2,1)}), bf16[128,2048]{1,0:T(8,128)(2,1)}) %reduce-scatter.2.cloned.1.call-update) | async-done | bytes 524304 | tf_op jit(solution)/shard_map/reduce_scatter | solution.py:223
  410.9 3.5 collective-permute-start.9
  414.4 24.2 %collective-permute-done.9 = bf16[128,2048]{1,0:T(8,128)(2,1)S(1)} collective-permute-done((bf16[128,2048]{1,0:T(8,128)(2,1)}, bf16[128,2048]{1,0:T(8,128)(2,1)S(1)}, u32[]{:S(2)}, u32[]{:S(2)}) %collective-permute-start.9) | collective-permute-done | bytes 524320 | tf_op jit(solution)/shard_map/ppermute | solution.py:25
  (91 shorter events, 24.9 us)
Async XLA Ops:
  6.5 44.1 %copy-start.16 = (bf16[256,512]{1,0:T(8,128)(2,1)S(1)}, bf16[256,512]{1,0:T(8,128)(2,1)}, u32[]{:S(2)}) copy-start(bf16[256,512]{1,0:T(8,128)(2,1)} %param.16) | copy-start | bytes 786436
  6.5 44.1 %copy-start.17 = (bf16[256,512]{1,0:T(8,128)(2,1)S(1)}, bf16[256,512]{1,0:T(8,128)(2,1)}, u32[]{:S(2)}) copy-start(bf16[256,512]{1,0:T(8,128)(2,1)} %param.17) | copy-start | bytes 786436
  6.5 44.1 %copy-start.10 = (bf16[256,1024]{1,0:T(8,128)(2,1)S(1)}, bf16[256,1024]{1,0:T(8,128)(2,1)}, u32[]{:S(2)}) copy-start(bf16[256,1024]{1,0:T(8,128)(2,1)} %param.18) | copy-start | bytes 1572868
  6.5 214.0 %all-gather.5.cloned.1.call-start = ((), (), s32[]{:S(2)}) async-start(), calls=%async_computation.1 | async-start | bytes 2621440 | tf_op jit(solution)/shard_map/all_gather | solution.py:175
  9.1 137.7 %copy-start.7 = (bf16[256,1024]{1,0:T(8,128)(2,1)S(1)}, bf16[256,1024]{1,0:T(8,128)(2,1)}, u32[]{:S(2)}) copy-start(bf16[256,1024]{1,0:T(8,128)(2,1)} %param.19) | copy-start | bytes 1572868
  9.1 137.7 %copy-start.13 = (bf16[256,512]{1,0:T(8,128)(2,1)S(1)}, bf16[256,512]{1,0:T(8,128)(2,1)}, u32[]{:S(2)}) copy-start(bf16[256,512]{1,0:T(8,128)(2,1)} %param.22) | copy-start | bytes 786436
  9.1 137.7 %copy-start.14 = (bf16[256,512]{1,0:T(8,128)(2,1)S(1)}, bf16[256,512]{1,0:T(8,128)(2,1)}, u32[]{:S(2)}) copy-start(bf16[256,512]{1,0:T(8,128)(2,1)} %param.21) | copy-start | bytes 786436
  9.1 40.6 %collective-permute-start = (bf16[128,2048]{1,0:T(8,128)(2,1)S(1)}, bf16[128,2048]{1,0:T(8,128)(2,1)S(1)}, u32[]{:S(2)}, u32[]{:S(2)}) collective-permute-start(bf16[128,2048]{1,0:T(8,128)(2,1)S(1)} %fusion.15), channel_id=1, source_target_pairs={{0,0},{1,8},{2,16},{3,24},{8,1},{9,9},{10,17},{11,25},{16,2},{17,1... | collective-permute-start | bytes 1572872 | tf_op jit(solution)/shard_map/ppermute | solution.py:25
  50.6 170.0 %all-gather.7.cloned.1.call-start = ((), (), s32[]{:S(2)}) async-start(), calls=%async_computation.2 | async-start | bytes 9437184 | tf_op jit(solution)/shard_map/all_gather | solution.py:182
  50.8 94.9 %collective-permute-start.1 = (bf16[256,2048]{1,0:T(8,128)(2,1)S(1)}, bf16[256,2048]{1,0:T(8,128)(2,1)S(1)}, u32[]{:S(2)}, u32[]{:S(2)}) collective-permute-start(bf16[256,2048]{1,0:T(8,128)(2,1)S(1)} %pad_maximum_fusion.1), channel_id=1, source_target_pairs={{0,0},{1,8},{2,16},{3,24},{8,1},{9,9},{10,17},{11,25},{16,2},{17,1... | collective-permute-start | bytes 3145736 | tf_op jit(solution)/shard_map/ppermute | solution.py:25
  145.7 1.0 copy-start.4
  146.8 31.2 %copy-start.8 = (bf16[256,1024]{1,0:T(8,128)(2,1)S(1)}, bf16[256,1024]{1,0:T(8,128)(2,1)}, u32[]{:S(2)}) copy-start(bf16[256,1024]{1,0:T(8,128)(2,1)} %param.26) | copy-start | bytes 1572868
  146.8 31.2 %copy-start.15 = (bf16[256,512]{1,0:T(8,128)(2,1)S(1)}, bf16[256,512]{1,0:T(8,128)(2,1)}, u32[]{:S(2)}) copy-start(bf16[256,512]{1,0:T(8,128)(2,1)} %param.27) | copy-start | bytes 786436
  146.8 177.3 %all-gather.9.cloned.1.call-start = ((), (), s32[]{:S(2)}) async-start(), calls=%async_computation.3 | async-start | bytes 11796480 | tf_op jit(solution)/shard_map/all_gather | solution.py:182
  148.0 28.9 %collective-permute-start.6 = (bf16[256,2560]{1,0:T(8,128)(2,1)S(1)}, bf16[256,2560]{1,0:T(8,128)(2,1)S(1)}, u32[]{:S(2)}, u32[]{:S(2)}) collective-permute-start(bf16[256,2560]{1,0:T(8,128)(2,1)S(1)} %pad_maximum_fusion), channel_id=1, source_target_pairs={{0,2},{1,10},{2,18},{3,26},{8,3},{9,11},{10,19},{11,27},{16,0},{17... | collective-permute-start | bytes 3932168 | tf_op jit(solution)/shard_map/ppermute | solution.py:35
  176.9 1.0 copy-start.1
  177.9 181.7 %all-gather.11.cloned.1.call-start = ((), (), s32[]{:S(2)}) async-start(), calls=%async_computation.4 | async-start | bytes 7077888 | tf_op jit(solution)/shard_map/all_gather | solution.py:182
  178.1 41.5 %collective-permute-start.8 = (bf16[256,1536]{1,0:T(8,128)(2,1)S(1)}, bf16[256,1536]{1,0:T(8,128)(2,1)S(1)}, u32[]{:S(2)}, u32[]{:S(2)}) collective-permute-start(bf16[256,1536]{1,0:T(8,128)(2,1)S(1)} %pad_maximum_fusion.2), channel_id=1, source_target_pairs={{0,0},{1,8},{2,16},{3,24},{8,1},{9,9},{10,17},{11,25},{16,2},{17,1... | collective-permute-start | bytes 2359304 | tf_op jit(solution)/shard_map/ppermute | solution.py:25
  193.6 35.5 %copy-start.18 = (f32[2]{0:T(128)}, f32[2]{0:T(128)S(1)}, u32[]{:S(2)}) copy-start(f32[2]{0:T(128)S(1)} %broadcast_multiply_fusion.2) | copy-start | bytes 28
  219.5 0.9 copy-start.6
  220.4 190.5 %reduce-scatter.2.cloned.1.call-start = ((), (), s32[]{:S(2)}) async-start(), calls=%async_computation.5 | async-start | bytes 2621440 | tf_op jit(solution)/shard_map/reduce_scatter | solution.py:223
  231.9 1.0 copy-start.2
  232.8 1.8 copy-start.3
  233.8 45.9 %copy-start.11 = (f32[512,2,128]{2,0,1:T(8,128)}, f32[512,2,128]{2,0,1:T(8,128)S(1)}, u32[]{:S(2)}) copy-start(f32[512,2,128]{2,0,1:T(8,128)S(1)} %get-tuple-element.11) | copy-start | bytes 1572868
  235.3 24.7 %collective-permute-start.2 = (bf16[2,256,512]{2,1,0:T(8,128)(2,1)S(1)}, bf16[2,256,512]{2,1,0:T(8,128)(2,1)S(1)}, u32[]{:S(2)}, u32[]{:S(2)}) collective-permute-start(bf16[2,256,512]{2,1,0:T(8,128)(2,1)S(1)} %convolution_convert_fusion.3), channel_id=1, source_target_pairs={{0,4},{4,1},{1,5},{5,2},{2,6},{6,3},{3,7},{8,12},{12,9},{9,13},{13... | collective-permute-start | bytes 1572872 | tf_op jit(solution)/shard_map/ppermute | solution.py:41
  260.0 18.7 %collective-permute-start.3 = (bf16[2,256,512]{2,1,0:T(8,128)(2,1)S(1)}, bf16[2,256,512]{2,1,0:T(8,128)(2,1)S(1)}, u32[]{:S(2)}, u32[]{:S(2)}) collective-permute-start(bf16[2,256,512]{2,1,0:T(8,128)(2,1)S(1)} %collective-permute-done.2), channel_id=1, source_target_pairs={{0,4},{4,1},{1,5},{5,2},{2,6},{6,3},{3,7},{8,12},{12,9},{9,13},{13... | collective-permute-start | bytes 1572872 | tf_op jit(solution)/shard_map/ppermute | solution.py:41
  279.8 26.0 %copy-start = (bf16[512,2048]{1,0:T(8,128)(2,1)S(1)}, bf16[512,2048]{1,0:T(8,128)(2,1)}, u32[]{:S(2)}) copy-start(bf16[512,2048]{1,0:T(8,128)(2,1)} %all-gather.5.cloned.1.call-done) | copy-start | bytes 6291460
  279.8 22.3 %collective-permute-start.4 = (bf16[2,256,512]{2,1,0:T(8,128)(2,1)}, bf16[2,256,512]{2,1,0:T(8,128)(2,1)}, u32[]{:S(2)}, u32[]{:S(2)}) collective-permute-start(bf16[2,256,512]{2,1,0:T(8,128)(2,1)} %fusion.30), channel_id=1, source_target_pairs={{0,1},{4,5},{1,2},{5,6},{2,3},{6,7},{8,9},{12,13},{9,10},{13,14},{... | collective-permute-start | bytes 1572872 | tf_op jit(solution)/shard_map/ppermute | solution.py:41
  304.3 13.5 %collective-permute-start.5 = (bf16[2,256,512]{2,1,0:T(8,128)(2,1)}, bf16[2,256,512]{2,1,0:T(8,128)(2,1)}, u32[]{:S(2)}, u32[]{:S(2)}) collective-permute-start(bf16[2,256,512]{2,1,0:T(8,128)(2,1)} %fusion.33), channel_id=1, source_target_pairs={{0,2},{4,6},{1,3},{5,7},{8,10},{12,14},{9,11},{13,15},{16,18},{20,... | collective-permute-start | bytes 1572872 | tf_op jit(solution)/shard_map/ppermute | solution.py:41
  321.9 2.3 copy-start.5
  333.3 7.5 %collective-permute-start.7 = (bf16[30,512]{1,0:T(8,128)(2,1)S(1)}, bf16[30,512]{1,0:T(8,128)(2,1)S(1)}, u32[]{:S(2)}, u32[]{:S(2)}) collective-permute-start(bf16[30,512]{1,0:T(8,128)(2,1)S(1)} %slice.278), channel_id=1, source_target_pairs={{0,4},{4,1},{1,5},{5,2},{2,6},{6,3},{3,7},{8,12},{12,9},{9,13},{13... | collective-permute-start | bytes 92168 | tf_op jit(solution)/shard_map/ppermute | solution.py:41
  410.9 27.7 %collective-permute-start.9 = (bf16[128,2048]{1,0:T(8,128)(2,1)}, bf16[128,2048]{1,0:T(8,128)(2,1)S(1)}, u32[]{:S(2)}, u32[]{:S(2)}) collective-permute-start(bf16[128,2048]{1,0:T(8,128)(2,1)} %reduce-scatter.2.cloned.1.call-done), channel_id=1, source_target_pairs={{0,0},{1,8},{2,16},{3,24},{8,1},{9,9},{10,17},{11,25},{16,2},{17,1... | collective-permute-start | bytes 1572872 | tf_op jit(solution)/shard_map/ppermute | solution.py:25
  (2 other events, 1.6 us)
Sparse Core Ops, SparseCore 0:
  50.7 62.1 all-gather.4
  146.9 71.9 all-gather.6
  220.8 87.3 all-gather.8
  309.9 49.6 all-gather.10
  367.2 43.6 reduce-scatter.1

commit v3 on v2

--- a/solution.py
+++ b/solution.py
@@ -1,6 +1,8 @@
 import jax
 import jax.numpy as jnp
 from jax import lax
+from jax.experimental import pallas as pl
+from jax.experimental.pallas import tpu as pltpu
 from jax.sharding import Mesh
 from jax.sharding import PartitionSpec as P
 
@@ -22,16 +24,6 @@
 def swap_planes(x):
     size = lax.axis_size("tp")
     pairs = [(h * size + t, t * size + h) for h in range(size) for t in range(size)]
-    return lax.ppermute(x, ("hi", "tp"), pairs)
-
-
-def swap_planes_rolled(x):
-    size = lax.axis_size("tp")
-    pairs = [
-        (h * size + t, t * size + (h + size // 2) % size)
-        for h in range(size)
-        for t in range(size)
-    ]
     return lax.ppermute(x, ("hi", "tp"), pairs)
 
 
@@ -50,6 +42,210 @@
         state = state + jnp.exp(log_span_decay * by)[:, None, None] * earlier
         by *= 2
     return state
+
+
+def spread_kernel(count, *refs):
+    rows_ref, blocks = refs[0], refs[1 : 1 + count]
+    tokens_out, fulls = refs[1 + count], refs[2 + count : 2 + 2 * count]
+    passing = refs[2 + 2 * count : 2 + 3 * count]
+    bounce = refs[2 + 3 * count : 2 + 4 * count]
+    rows_bounce, send, arrive, arrive_pass, send_rows, arrive_rows, own = refs[2 + 4 * count :]
+    hi, lo, tp = lax.axis_index("hi"), lax.axis_index("lo"), lax.axis_index("tp")
+    planes = lax.axis_size("hi")
+    side, core = tp // 2, tp % 2
+    far_side = 1 - side
+    across = (hi, lo, 2 * far_side + core)
+    beside = (hi, 1 - lo, tp)
+    sibling = (hi, lo, 2 * side + 1 - core)
+    held = lax.rem(side + hi // 2, 2)
+    other_held = 1 - held
+
+    def remote(source, target, out_sem, in_sem, device):
+        return pltpu.make_async_remote_copy(
+            src_ref=source,
+            dst_ref=target,
+            send_sem=out_sem,
+            recv_sem=in_sem,
+            device_id=device,
+            device_id_type=pl.DeviceIdType.MESH,
+        )
+
+    def via_vmem(source, buffer, target, done):
+        inward = pltpu.make_async_copy(source, buffer, own)
+        inward.start()
+        inward.wait()
+        pltpu.make_async_copy(buffer, target, done).start()
+
+    def piece(k, source, row, half):
+        depth = blocks[k].shape[0]
+        start = (source * 2 + row) * depth + half * (depth // 2)
+        return fulls[k].at[pl.ds(pl.multiple_of(start, depth // 2), depth // 2)]
+
+    def half_of(k, half):
+        depth = blocks[k].shape[0] // 2
+        return blocks[k].at[pl.ds(half * depth, depth)]
+
+    waits = []
+
+    def push(k, source, row, half, slot, device):
+        part = piece(k, source, row, half)
+        copy = remote(part, part, send.at[k, slot], arrive.at[k, source, row, half], device)
+        copy.start()
+        waits.append(copy)
+
+    def landed(k, source, row, half):
+        part = piece(k, source, row, half)
+        remote(part, part, send.at[k, 0], arrive.at[k, source, row, half], across).wait_recv()
+
+    landing = pl.multiple_of(tp * rows_ref.shape[0], rows_ref.shape[0])
+    my_rows = tokens_out.at[pl.ds(landing, rows_ref.shape[0])]
+
+    for k in range(count):
+        copy = remote(half_of(k, 1), passing[k], send.at[k, 0], arrive_pass.at[k], across)
+        copy.start()
+        waits.append(copy)
+
+    def first_entry(k):
+        return remote(
+            half_of(k, 0),
+            piece(k, hi, lo, 0),
+            send.at[k, 1],
+            arrive.at[k, hi, lo, 0],
+            (tp, lo, 2 * side + lax.rem(hi, 2)),
+        )
+
+    def second_entry(k):
+        return remote(
+            passing[k],
+            piece(k, hi, lo, 1),
+            send.at[k, 2],
+            arrive.at[k, hi, lo, 1],
+            (2 * far_side + core, lo, 2 * side + lax.rem(hi, 2)),
+        )
+
+    def rows_copy(step):
+        target = lax.rem(hi + step, planes)
+        return remote(
+            rows_ref, my_rows, send_rows.at[step], arrive_rows.at[tp], (target, lo, hi)
+        )
+
+    stays_first = tp == hi
+    stays_second = 2 * far_side + core == hi
+    for k in range(count):
+
+        @pl.when(jnp.logical_not(stays_first))
+        def _():
+            first_entry(k).start()
+
+    for step in range(1, 4):
+        rows_copy(step).start()
+
+    @pl.when(jnp.logical_not(stays_first))
+    def _():
+        rows_copy(0).start()
+
+    @pl.when(stays_first)
+    def _():
+        via_vmem(rows_ref, rows_bounce, my_rows, arrive_rows.at[tp])
+        for k in range(count):
+            via_vmem(half_of(k, 0), bounce[k], piece(k, hi, lo, 0), arrive.at[k, hi, lo, 0])
+
+    for k in range(count):
+        remote(passing[k], passing[k], send.at[k, 0], arrive_pass.at[k], across).wait_recv()
+
+        @pl.when(jnp.logical_not(stays_second))
+        def _():
+            second_entry(k).start()
+
+        @pl.when(stays_second)
+        def _():
+            via_vmem(passing[k], bounce[k], piece(k, hi, lo, 1), arrive.at[k, hi, lo, 1])
+
+    def own_step(k):
+        for n in range(2):
+            source = core + 2 * n
+            landed(k, source, lo, held)
+            push(k, source, lo, held, 3 + 3 * n, across)
+            push(k, source, lo, held, 4 + 3 * n, beside)
+            push(k, source, lo, held, 5 + 3 * n, sibling)
+
+    def near_step(k):
+        landed(k, core, lo, other_held)
+        push(k, core, lo, other_held, 9, beside)
+        push(k, core, lo, other_held, 10, sibling)
+        landed(k, core + 2, 1 - lo, held)
+        push(k, core + 2, 1 - lo, held, 11, across)
+        push(k, core + 2, 1 - lo, held, 12, sibling)
+        landed(k, core + 2, lo, other_held)
+        push(k, core + 2, lo, other_held, 13, sibling)
+        landed(k, core, 1 - lo, held)
+        push(k, core, 1 - lo, held, 14, sibling)
+
+    def far_step(k):
+        landed(k, core, 1 - lo, other_held)
+        push(k, core, 1 - lo, other_held, 15, sibling)
+        landed(k, core + 2, 1 - lo, other_held)
+        push(k, core + 2, 1 - lo, other_held, 16, sibling)
+
+    for step in range(count + 2):
+        if step < count:
+            own_step(step)
+        if 0 <= step - 1 < count:
+            near_step(step - 1)
+        if 0 <= step - 2:
+            far_step(step - 2)
+
+    for k in range(count):
+        for n in range(2):
+            for row in range(2):
+                for half in range(2):
+                    landed(k, 1 - core + 2 * n, row, half)
+    for t in range(4):
+        part = tokens_out.at[pl.ds(t * rows_ref.shape[0], rows_ref.shape[0])]
+        remote(part, part, send_rows.at[0], arrive_rows.at[t], across).wait_recv()
+    for copy in waits:
+        copy.wait_send()
+    for step in range(1, 4):
+        rows_copy(step).wait_send()
+
+    @pl.when(jnp.logical_not(stays_first))
+    def _():
+        rows_copy(0).wait_send()
+        for k in range(count):
+            first_entry(k).wait_send()
+
+    @pl.when(jnp.logical_not(stays_second))
+    def _():
+        for k in range(count):
+            second_entry(k).wait_send()
+
+
+def spread(rows, blocks):
+    count = len(blocks)
+    shares = lax.axis_size(SPANS)
+    halves = [(b.shape[0] // 2, b.shape[1]) for b in blocks]
+    outs = [jax.ShapeDtypeStruct((4 * rows.shape[0], rows.shape[1]), rows.dtype)]
+    outs += [jax.ShapeDtypeStruct((shares * b.shape[0], b.shape[1]), b.dtype) for b in blocks]
+    outs += [jax.ShapeDtypeStruct(h, b.dtype) for h, b in zip(halves, blocks)]
+    results = pl.pallas_call(
+        lambda *refs: spread_kernel(count, *refs),
+        out_shape=outs,
+        in_specs=[pl.BlockSpec(memory_space=pl.ANY)] * (1 + count),
+        out_specs=[pl.BlockSpec(memory_space=pl.ANY)] * len(outs),
+        scratch_shapes=[pltpu.VMEM(h, b.dtype) for h, b in zip(halves, blocks)]
+        + [
+            pltpu.VMEM(rows.shape, rows.dtype),
+            pltpu.SemaphoreType.DMA((count, 17)),
+            pltpu.SemaphoreType.DMA((count, 4, 2, 2)),
+            pltpu.SemaphoreType.DMA((count,)),
+            pltpu.SemaphoreType.DMA((4,)),
+            pltpu.SemaphoreType.DMA((4,)),
+            pltpu.SemaphoreType.DMA,
+        ],
+        compiler_params=pltpu.CompilerParams(has_side_effects=True),
+        name="spread",
+    )(rows, *blocks)
+    return results[0], results[1 : 1 + count]
 
 
 def rms_normalize(tokens, norm_gain):
@@ -172,17 +368,6 @@
     chain_length = lax.axis_size(SPANS)
     head_rank = lax.axis_index("hi")
     chain_rank = lax.axis_index(SPANS)
-    normed = lax.all_gather(
-        swap_planes(rms_normalize(tokens, norm_gain)), "hi", axis=0, tiled=True
-    )
-    half = normed.shape[1] // 2
-    normed_rolled = jnp.concatenate([normed[:, half:], normed[:, :half]], axis=1)
-
-    def gathered(swap, *matrices):
-        return lax.all_gather(
-            swap(jnp.concatenate(matrices, axis=1)), SPANS, axis=0, tiled=True
-        )
-
     def project(rows, merged, *matrices):
         product = jnp.dot(rows, merged, preferred_element_type=jnp.float32).astype(jnp.bfloat16)
         ends = [sum(m.shape[1] for m in matrices[: k + 1]) for k in range(len(matrices) - 1)]
@@ -191,11 +376,17 @@
     first = (key_weight, value_weight, query_weight)
     second = (unit_value, unit_gate, convolve_gate, retain_gate)
     third = (retain_output, convolve_output)
-    key_rows, values, queries = project(normed, gathered(swap_planes, *first), *first)
-    glu_value, glu_switch, convolve_switch, retain_switch = project(
-        normed_rolled, gathered(swap_planes_rolled, *second), *second
-    )
-    out_full = gathered(swap_planes, *third)
+    groups = (first, second, third)
+    merged = [jnp.concatenate(group, axis=1) for group in groups]
+    normed = rms_normalize(tokens, norm_gain)
+    if (lax.axis_size("lo"), lax.axis_size("tp")) == (2, 4):
+        normed, merged = spread(normed, merged)
+    else:
+        normed = lax.all_gather(swap_planes(normed), "hi", axis=0, tiled=True)
+        merged = [lax.all_gather(swap_planes(m), SPANS, axis=0, tiled=True) for m in merged]
+    key_rows, values, queries = project(normed, merged[0], *first)
+    glu_value, glu_switch, convolve_switch, retain_switch = project(normed, merged[1], *second)
+    out_full = merged[2]
     row_count = normed.shape[0]
     local_heads = queries.shape[1] // KEY
     positions = chain_rank * row_count + jnp.arange(row_count, dtype=jnp.int32)

time: 447 us -> 373 us (0.83)
  waiting for transfers between devices: 316 us -> 89.9 us
  Pallas kernels: 0 us -> 179 us
  starting transfers between devices: 47.2 us -> 17.6 us
    pallas_call x0 -> x1, Pallas kernels: none -> 179 us  [spread(): pl.pallas_call(lambda *refs: spread_kernel(count, *refs), out_shape=outs,...]
    ppermute x4 -> x1, waiting for transfers between devices: 177 us -> 24.3 us  [swap_planes(): return lax.ppermute(x, ('hi', 'tp'), pairs)]
    ppermute x5, waiting for transfers between devices: 52.8 us -> 12.8 us  [from_behind(): return lax.ppermute(x, ('lo', 'tp'), list(zip(spot[:-by], spot[by:])))]
    ppermute x1 -> x0, waiting for transfers between devices: 28.8 us -> none  [swap_planes_rolled(): return lax.ppermute(x, ('hi', 'tp'), pairs)]
    ppermute x4 -> x1, starting transfers between devices: 25.5 us -> 3.51 us  [swap_planes(): return lax.ppermute(x, ('hi', 'tp'), pairs)]
    all_gather x4 -> x0, waiting for transfers between devices: 13.4 us -> none  [the longest x3 13.4 us: gathered(): lax.all_gather(swap(jnp.concatenate(matrices, axis=1)), SPANS, axis=0, ti...]
    reduce_scatter x1, waiting for transfers between devices: 43.8 us -> 52.8 us  [local(): lax.psum_scatter(mixed, 'hi', scatter_dimension=0, tiled=True)]
    ppermute x5, starting transfers between devices: 21.5 us -> 14 us  [from_behind(): return lax.ppermute(x, ('lo', 'tp'), list(zip(spot[:-by], spot[by:])))]
  transfers between devices with their start and end apart: 15 -> 7, of which waited for: 12 -> 5; matrix products, arithmetic and copies ran while one was open for 12% -> 9% of each run, Pallas kernels for 0% -> 0%
where the time goes in v3:
time: 373 us; the launch traced here: 372 us
  Pallas kernels  179 us (48%)
  waiting for transfers between devices  89.9 us (24%)
  matrix products  32.6 us (9%)
  other arithmetic  25.8 us (7%)
  starting transfers between devices  17.6 us (5%)
  between operations  13.8 us (4%)
  local copies, waits for them, and re-layouts  12.4 us (3%)
    pallas_call x1, Pallas kernels, spread(): pl.pallas_call(lambda *refs: spread_kernel(count, *refs), out_shape=outs,...  179 us
    reduce_scatter x1, waiting for transfers between devices, local(): lax.psum_scatter(mixed, 'hi', scatter_dimension=0, tiled=True)  52.8 us
    ppermute x1, waiting for transfers between devices, swap_planes(): return lax.ppermute(x, ('hi', 'tp'), pairs)  24.3 us
    dot_general x2, matrix products, project(): jnp.dot(rows, merged, preferred_element_type=jnp.float32)  19.4 us
    ppermute x5, starting transfers between devices, from_behind(): return lax.ppermute(x, ('lo', 'tp'), list(zip(spot[:-by], spot[by:])))  14 us
    ppermute x5, waiting for transfers between devices, from_behind(): return lax.ppermute(x, ('lo', 'tp'), list(zip(spot[:-by], spot[by:])))  12.8 us
  transfers between devices with their start and end apart: 7, of which 5 were waited for; matrix products, arithmetic and copies ran while one was open for 9% of the time, Pallas kernels for 0%

profile of v3, /device:TPU:2, one launch (start us, length us, event | category | flops | bytes accessed | tf_op | source)
XLA Modules:
  0.0 371.6 jit_solution(10417067874516821925)
XLA Ops:
  6.6 1.3 fusion.10
  8.0 2.2 pad_maximum_fusion.2.refs_3_
  11.2 1.1 pad_maximum_fusion.1.refs_1_
  12.3 1.1 pad_maximum_fusion.refs_2_
  13.5 179.5 %spread.1 = (bf16[512,2048]{1,0:T(8,128)(2,1)}, bf16[2048,2048]{1,0:T(8,128)(2,1)}, bf16[2048,2560]{1,0:T(8,128)(2,1)}, bf16[2048,1536]{1,0:T(8,128)(2,1)}, bf16...) custom-call(bf16[128,2048]{1,0:T(8,128)(2,1)} %fusion.12.refs_0_, ...), custom_call_target="tpu_custom_call" | custom-call | tf_op jit(solution)/shard_map/spread/pallas_call | solution.py:230
  192.9 8.5 %convolution_convert_fusion.2 = bf16[512,2048]{1,0:T(8,128)(2,1)S(1)} fusion(bf16[512,2048]{1,0:T(8,128)(2,1)} %get-tuple-element.9, bf16[2048,2048]{1,0:T(8,128)(2,1)} %get-tuple-element.10), kind=kOutput, calls=%fused_computation.31 | convolution fusion | flops 4296015872 | bytes 12582912 | tf_op jit(solution)/shard_map/dot_general | solution.py:372
  201.7 1.1 split.28
  205.0 1.0 multiply_cosine_fusion
  208.0 2.4 collective-permute-start
  210.4 10.9 %convolution_convert_fusion = bf16[512,2560]{1,0:T(8,128)(2,1)} fusion(bf16[512,2048]{1,0:T(8,128)(2,1)S(1)} %copy-done.20, bf16[2048,2560]{1,0:T(8,128)(2,1)} %get-tuple-element.11), kind=kOutput, calls=%fused_computation.29 | convolution fusion | flops 5370019840 | bytes 15204352 | tf_op jit(solution)/shard_map/dot_general | solution.py:372
  221.4 1.5 multiply_convert_fusion.1
  222.9 3.6 collective-permute-start.4
  227.6 1.2 fusion.81
  228.8 1.8 constant_dynamic-slice_fusion
  231.0 2.2 collective-permute-start.1
  233.7 1.3 dynamic_slice.10
  235.1 1.3 dynamic_slice.11
  236.4 1.2 fusion.23
  237.6 4.2 %fusion.9 = f32[2,512,512]{2,1,0:T(8,128)} fusion(f32[512,512]{1,0:T(8,128)} %fusion.23, f32[2]{0:T(128)} %copy-done.19, pred[512,512]{1,0:T(8,128)(4,1)S(1)} %fusion.24, bf16[64,2,8,512]{3,2,1,0:T(8,128)(2,1)S(1)} %bitcast.51, bf16[512,2,128]{2,0,1:T(8,128)(2,1)S(1)} %get-tuple-element.25, bf16[512,2,128]{2,0,1:T(8,128)(2,1)S(1)} %get-tuple-element.26, ...), kind=kOutput, calls=%fused_computation.47 | convolution fusion | flops 809238528 | bytes 6029320 | tf_op jit(solution)/shard_map/hij,jhe->ihe/dot_general | solution.py:299
  241.8 1.4 collective-permute-done.1
  244.0 4.5 %collective-permute-start.2 = (bf16[2,256,512]{2,1,0:T(8,128)(2,1)S(1)}, bf16[2,256,512]{2,1,0:T(8,128)(2,1)S(1)}, u32[]{:S(2)}, u32[]{:S(2)}) collective-permute-start(bf16[2,256,512]{2,1,0:T(8,128)(2,1)S(1)} %fusion.27), channel_id=1, source_target_pairs={{0,1},{4,5},{1,2},{5,6},{2,3},{6,7},{8,9},{12,13},{9,10},{13,14},{... | collective-permute-start | bytes 1572872 | tf_op jit(solution)/shard_map/ppermute | solution.py:33
  248.5 5.6 %fusion.78 = (f32[512]{0:T(512)S(1)}, f32[512,512]{1,0:T(8,128)S(1)}) fusion(f32[512]{0:T(512)S(1)} %bitcast.64, bf16[512,512]{1,0:T(8,128)(2,1)S(1)} %multiply_convert_fusion.1, f32[512]{0:T(512)S(1)} %bitcast.66, bf16[30,512]{1,0:T(8,128)(2,1)S(1)} %collective-permute-done.4, f32[512]{0:T(512)S(1)} %bitcast.67, f32[512]{0:T(512)S(1)} %bitcast.68, ...), kind=kLoop, calls=%fused_computation.159 | loop fusion | flops 47971840 | bytes 1669120 | tf_op jit(solution)/shard_map/reduce_sum | solution.py:338
  254.4 1.1 collective-permute-done.2
  255.9 1.3 collective-permute-start.3
  257.2 2.5 fusion.25
  259.7 10.3 %collective-permute-done.3 = bf16[2,256,512]{2,1,0:T(8,128)(2,1)S(1)} collective-permute-done((bf16[2,256,512]{2,1,0:T(8,128)(2,1)S(1)}, bf16[2,256,512]{2,1,0:T(8,128)(2,1)S(1)}, u32[]{:S(2)}, u32[]{:S(2)}) %collective-permute-start.3) | collective-permute-done | bytes 524320 | tf_op jit(solution)/shard_map/ppermute | solution.py:33
  271.6 1.8 copy.23
  273.4 2.6 fusion.5
  276.0 7.4 %convolution_convert_fusion.1 = bf16[512,2048]{1,0:T(8,128)(2,1)} fusion(bf16[2048,1536]{1,0:T(8,128)(2,1)} %get-tuple-element.12, bf16[512,512]{1,0:T(8,128)(2,1)S(1)} %copy-done.5, bf16[512,1024]{1,0:T(8,128)(2,1)S(1)} %fusion.5), kind=kOutput, calls=%fused_computation.30 | convolution fusion | flops 3225419776 | bytes 9961472 | tf_op jit(solution)/shard_map/dot_general | solution.py:346
  283.4 52.8 %reduce-scatter.2.cloned.1.call-done = bf16[128,2048]{1,0:T(8,128)(2,1)} async-done(((bf16[512,2048]{1,0:T(8,128)(2,1)}), bf16[128,2048]{1,0:T(8,128)(2,1)}) %reduce-scatter.2.cloned.1.call-update) | async-done | bytes 524304 | tf_op jit(solution)/shard_map/reduce_scatter | solution.py:414
  336.2 3.5 collective-permute-start.5
  339.8 24.3 %collective-permute-done.5 = bf16[128,2048]{1,0:T(8,128)(2,1)S(1)} collective-permute-done((bf16[128,2048]{1,0:T(8,128)(2,1)}, bf16[128,2048]{1,0:T(8,128)(2,1)S(1)}, u32[]{:S(2)}, u32[]{:S(2)}) %collective-permute-start.5) | collective-permute-done | bytes 524320 | tf_op jit(solution)/shard_map/ppermute | solution.py:27
  (75 shorter events, 11.1 us)
Async XLA Ops:
  6.5 3.6 copy-start.1
  6.5 3.6 copy-start.13
  6.5 4.6 %copy-start.11 = (bf16[256,512]{1,0:T(8,128)(2,1)S(1)}, bf16[256,512]{1,0:T(8,128)(2,1)}, u32[]{:S(2)}) copy-start(bf16[256,512]{1,0:T(8,128)(2,1)} %param.16) | copy-start | bytes 786436
  6.5 4.6 %copy-start.12 = (bf16[256,512]{1,0:T(8,128)(2,1)S(1)}, bf16[256,512]{1,0:T(8,128)(2,1)}, u32[]{:S(2)}) copy-start(bf16[256,512]{1,0:T(8,128)(2,1)} %param.17) | copy-start | bytes 786436
  6.5 4.6 %copy-start.4 = (bf16[256,1024]{1,0:T(8,128)(2,1)S(1)}, bf16[256,1024]{1,0:T(8,128)(2,1)}, u32[]{:S(2)}) copy-start(bf16[256,1024]{1,0:T(8,128)(2,1)} %param.18) | copy-start | bytes 1572868
  6.5 329.7 %reduce-scatter.2.cloned.1.call-start = ((), (), s32[]{:S(2)}) async-start(), calls=%async_computation.1 | async-start | bytes 2621440 | tf_op jit(solution)/shard_map/reduce_scatter | solution.py:414
  8.0 4.3 %copy-start.3 = (bf16[256,1024]{1,0:T(8,128)(2,1)S(1)}, bf16[256,1024]{1,0:T(8,128)(2,1)}, u32[]{:S(2)}) copy-start(bf16[256,1024]{1,0:T(8,128)(2,1)} %param.19) | copy-start | bytes 1572868
  8.0 4.3 %copy-start.8 = (bf16[256,512]{1,0:T(8,128)(2,1)S(1)}, bf16[256,512]{1,0:T(8,128)(2,1)}, u32[]{:S(2)}) copy-start(bf16[256,512]{1,0:T(8,128)(2,1)} %param.22) | copy-start | bytes 786436
  8.0 4.3 %copy-start.9 = (bf16[256,512]{1,0:T(8,128)(2,1)S(1)}, bf16[256,512]{1,0:T(8,128)(2,1)}, u32[]{:S(2)}) copy-start(bf16[256,512]{1,0:T(8,128)(2,1)} %param.21) | copy-start | bytes 786436
  8.0 4.3 %copy-start.10 = (bf16[256,512]{1,0:T(8,128)(2,1)S(1)}, bf16[256,512]{1,0:T(8,128)(2,1)}, u32[]{:S(2)}) copy-start(bf16[256,512]{1,0:T(8,128)(2,1)} %param.20) | copy-start | bytes 786436
  204.2 1.7 copy-start.19
  206.1 1.2 copy-start.2
  206.4 0.8 copy-start.6
  206.4 1.6 copy-start.7
  206.4 4.0 %copy-start.20 = (bf16[512,2048]{1,0:T(8,128)(2,1)S(1)}, bf16[512,2048]{1,0:T(8,128)(2,1)}, u32[]{:S(2)}) copy-start(bf16[512,2048]{1,0:T(8,128)(2,1)} %get-tuple-element.9) | copy-start | bytes 6291460
  208.0 23.0 %collective-permute-start = (bf16[2,256,512]{2,1,0:T(8,128)(2,1)S(1)}, bf16[2,256,512]{2,1,0:T(8,128)(2,1)S(1)}, u32[]{:S(2)}, u32[]{:S(2)}) collective-permute-start(bf16[2,256,512]{2,1,0:T(8,128)(2,1)S(1)} %convolution_convert_fusion.3), channel_id=1, source_target_pairs={{0,4},{4,1},{1,5},{5,2},{2,6},{6,3},{3,7},{8,12},{12,9},{9,13},{13... | collective-permute-start | bytes 1572872 | tf_op jit(solution)/shard_map/ppermute | solution.py:33
  222.9 25.6 %collective-permute-start.4 = (bf16[30,512]{1,0:T(8,128)(2,1)S(1)}, bf16[30,512]{1,0:T(8,128)(2,1)S(1)}, u32[]{:S(2)}, u32[]{:S(2)}) collective-permute-start(bf16[30,512]{1,0:T(8,128)(2,1)S(1)} %slice.268), channel_id=1, source_target_pairs={{0,4},{4,1},{1,5},{5,2},{2,6},{6,3},{3,7},{8,12},{12,9},{9,13},{13... | collective-permute-start | bytes 92168 | tf_op jit(solution)/shard_map/ppermute | solution.py:33
  231.0 12.2 %collective-permute-start.1 = (bf16[2,256,512]{2,1,0:T(8,128)(2,1)S(1)}, bf16[2,256,512]{2,1,0:T(8,128)(2,1)S(1)}, u32[]{:S(2)}, u32[]{:S(2)}) collective-permute-start(bf16[2,256,512]{2,1,0:T(8,128)(2,1)S(1)} %collective-permute-done), channel_id=1, source_target_pairs={{0,4},{4,1},{1,5},{5,2},{2,6},{6,3},{3,7},{8,12},{12,9},{9,13},{13... | collective-permute-start | bytes 1572872 | tf_op jit(solution)/shard_map/ppermute | solution.py:33
  241.8 13.8 %copy-start.16 = (f32[2]{0:T(128)S(1)}, f32[2]{0:T(128)}, u32[]{:S(2)}) copy-start(f32[2]{0:T(128)} %multiply_exponential_fusion.4) | copy-start | bytes 28
  241.8 13.8 %copy-start.17 = (f32[2]{0:T(128)S(1)}, f32[2]{0:T(128)}, u32[]{:S(2)}) copy-start(f32[2]{0:T(128)} %multiply_exponential_fusion.3) | copy-start | bytes 28
  244.0 11.5 %collective-permute-start.2 = (bf16[2,256,512]{2,1,0:T(8,128)(2,1)S(1)}, bf16[2,256,512]{2,1,0:T(8,128)(2,1)S(1)}, u32[]{:S(2)}, u32[]{:S(2)}) collective-permute-start(bf16[2,256,512]{2,1,0:T(8,128)(2,1)S(1)} %fusion.27), channel_id=1, source_target_pairs={{0,1},{4,5},{1,2},{5,6},{2,3},{6,7},{8,9},{12,13},{9,10},{13,14},{... | collective-permute-start | bytes 1572872 | tf_op jit(solution)/shard_map/ppermute | solution.py:33
  248.5 8.7 %copy-start.14 = (f32[512]{0:T(512)S(1)}, f32[512]{0:T(512)}, u32[]{:S(2)}) copy-start(f32[512]{0:T(512)} %dynamic_slice.10) | copy-start | bytes 6148
  248.5 8.7 %copy-start.15 = (f32[512]{0:T(512)S(1)}, f32[512]{0:T(512)}, u32[]{:S(2)}) copy-start(f32[512]{0:T(512)} %dynamic_slice.11) | copy-start | bytes 6148
  254.4 15.7 %copy-start = (f32[2,512,512]{2,1,0:T(8,128)S(1)}, f32[2,512,512]{2,1,0:T(8,128)}, u32[]{:S(2)}) copy-start(f32[2,512,512]{2,1,0:T(8,128)} %fusion.9) | copy-start | bytes 6291460
  254.4 15.6 %copy-start.18 = (f32[2]{0:T(128)S(1)}, f32[2]{0:T(128)}, u32[]{:S(2)}) copy-start(f32[2]{0:T(128)} %multiply_exponential_fusion.2) | copy-start | bytes 28
  255.9 14.1 %collective-permute-start.3 = (bf16[2,256,512]{2,1,0:T(8,128)(2,1)S(1)}, bf16[2,256,512]{2,1,0:T(8,128)(2,1)S(1)}, u32[]{:S(2)}, u32[]{:S(2)}) collective-permute-start(bf16[2,256,512]{2,1,0:T(8,128)(2,1)S(1)} %fusion.30), channel_id=1, source_target_pairs={{0,2},{4,6},{1,3},{5,7},{8,10},{12,14},{9,11},{13,15},{16,18},{20,... | collective-permute-start | bytes 1572872 | tf_op jit(solution)/shard_map/ppermute | solution.py:33
  273.4 2.6 copy-start.5
  336.2 27.8 %collective-permute-start.5 = (bf16[128,2048]{1,0:T(8,128)(2,1)}, bf16[128,2048]{1,0:T(8,128)(2,1)S(1)}, u32[]{:S(2)}, u32[]{:S(2)}) collective-permute-start(bf16[128,2048]{1,0:T(8,128)(2,1)} %reduce-scatter.2.cloned.1.call-done), channel_id=1, source_target_pairs={{0,0},{1,8},{2,16},{3,24},{8,1},{9,9},{10,17},{11,25},{16,2},{17,1... | collective-permute-start | bytes 1572872 | tf_op jit(solution)/shard_map/ppermute | solution.py:27
Sparse Core Ops, SparseCore 0:
  283.6 52.6 reduce-scatter.1

commit v4 on v3

--- a/solution.py
+++ b/solution.py
@@ -173,11 +173,14 @@
         landed(k, core, lo, other_held)
         push(k, core, lo, other_held, 9, beside)
         push(k, core, lo, other_held, 10, sibling)
+        landed(k, core + 2, lo, other_held)
+        if k < count - 1:
+            push(k, core + 2, lo, other_held, 11, beside)
+        push(k, core + 2, lo, other_held, 12, sibling)
         landed(k, core + 2, 1 - lo, held)
-        push(k, core + 2, 1 - lo, held, 11, across)
-        push(k, core + 2, 1 - lo, held, 12, sibling)
-        landed(k, core + 2, lo, other_held)
-        push(k, core + 2, lo, other_held, 13, sibling)
+        if k == count - 1:
+            push(k, core + 2, 1 - lo, held, 11, across)
+        push(k, core + 2, 1 - lo, held, 13, sibling)
         landed(k, core, 1 - lo, held)
         push(k, core, 1 - lo, held, 14, sibling)
 
@@ -373,10 +376,14 @@
         ends = [sum(m.shape[1] for m in matrices[: k + 1]) for k in range(len(matrices) - 1)]
         return jnp.split(product, ends, axis=1)
 
-    first = (key_weight, value_weight, query_weight)
-    second = (unit_value, unit_gate, convolve_gate, retain_gate)
-    third = (retain_output, convolve_output)
-    groups = (first, second, third)
+    groups = (
+        (key_weight, query_weight),
+        (value_weight,),
+        (unit_value, unit_gate),
+        (retain_gate,),
+        (convolve_gate, convolve_output),
+        (retain_output,),
+    )
     merged = [jnp.concatenate(group, axis=1) for group in groups]
     normed = rms_normalize(tokens, norm_gain)
     if (lax.axis_size("lo"), lax.axis_size("tp")) == (2, 4):
@@ -384,9 +391,13 @@
     else:
         normed = lax.all_gather(swap_planes(normed), "hi", axis=0, tiled=True)
         merged = [lax.all_gather(swap_planes(m), SPANS, axis=0, tiled=True) for m in merged]
-    key_rows, values, queries = project(normed, merged[0], *first)
-    glu_value, glu_switch, convolve_switch, retain_switch = project(normed, merged[1], *second)
-    out_full = merged[2]
+    key_rows, queries = project(normed, merged[0], *groups[0])
+    (values,) = project(normed, merged[1], *groups[1])
+    glu_value, glu_switch = project(normed, merged[2], *groups[2])
+    (retain_switch,) = project(normed, merged[3], *groups[3])
+    gate_full, convolve_full = jnp.split(merged[4], [convolve_gate.shape[1]], axis=1)
+    (convolve_switch,) = project(normed, gate_full, convolve_gate)
+    retain_full = merged[5]
     row_count = normed.shape[0]
     local_heads = queries.shape[1] // KEY
     positions = chain_rank * row_count + jnp.arange(row_count, dtype=jnp.int32)
@@ -409,8 +420,9 @@
     convolve_hidden = convolve_branch(
         gated_input, before, tap_slice, gain_slice, shift_slice, convolve_switch
     )
-    hidden = jnp.concatenate([retain_hidden, convolve_hidden], axis=1)
-    mixed = contract(hidden, out_full).astype(jnp.bfloat16)
+    mixed = (
+        contract(retain_hidden, retain_full) + contract(convolve_hidden, convolve_full)
+    ).astype(jnp.bfloat16)
     return swap_planes(lax.psum_scatter(mixed, "hi", scatter_dimension=0, tiled=True))
 
 

time: 373 us -> 395 us (1.059)
  Pallas kernels: 179 us -> 209 us
  other arithmetic: 25.8 us -> 18.2 us
  waiting for transfers between devices: 89.9 us -> 85.6 us
  matrix products: 32.6 us -> 36.9 us
    pallas_call x1, Pallas kernels: 179 us -> 209 us  [spread(): pl.pallas_call(lambda *refs: spread_kernel(count, *refs), out_shape=outs,...]
    dot_general x1 -> x2, matrix products: 7.43 us -> 19 us  [contract(): lax.dot_general(hidden, matrix, (((1,), (1,)), ((), ())), preferred_eleme...]
    reduce_scatter x1, waiting for transfers between devices: 52.8 us -> 42.7 us  [local(): lax.psum_scatter(mixed, 'hi', scatter_dimension=0, tiled=True)]
    dot_general x2 -> x3, matrix products: 19.4 us -> 12.1 us  [project(): jnp.dot(rows, merged, preferred_element_type=jnp.float32)]
    ppermute x5, waiting for transfers between devices: 12.8 us -> 18.6 us  [from_behind(): return lax.ppermute(x, ('lo', 'tp'), list(zip(spot[:-by], spot[by:])))]
    convert_element_type x2 -> x0, other arithmetic: 5.09 us -> none  [the longest x1 2.61 us: retain_finish(): (normalized * jax.nn.silu(switch.astype(jnp.float32))).astype(jnp.bfloat16)]
  transfers between devices with their start and end apart: 7 -> 7, of which waited for: 5 -> 6; matrix products, arithmetic and copies ran while one was open for 9% -> 5% of each run, Pallas kernels for 0% -> 0%
where the time goes in v4:
time: 395 us; the launch traced here: 394 us
  Pallas kernels  209 us (53%)
  waiting for transfers between devices  85.6 us (22%)
  matrix products  36.9 us (9%)
  starting transfers between devices  18.4 us (5%)
  other arithmetic  18.2 us (5%)
  between operations  13.8 us (3%)
  local copies, waits for them, and re-layouts  12.8 us (3%)
    pallas_call x1, Pallas kernels, spread(): pl.pallas_call(lambda *refs: spread_kernel(count, *refs), out_shape=outs,...  209 us
    reduce_scatter x1, waiting for transfers between devices, local(): lax.psum_scatter(mixed, 'hi', scatter_dimension=0, tiled=True)  42.7 us
    ppermute x1, waiting for transfers between devices, swap_planes(): return lax.ppermute(x, ('hi', 'tp'), pairs)  24.2 us
    dot_general x2, matrix products, contract(): lax.dot_general(hidden, matrix, (((1,), (1,)), ((), ())), preferred_eleme...  19 us
    ppermute x5, waiting for transfers between devices, from_behind(): return lax.ppermute(x, ('lo', 'tp'), list(zip(spot[:-by], spot[by:])))  18.6 us
    ppermute x5, starting transfers between devices, from_behind(): return lax.ppermute(x, ('lo', 'tp'), list(zip(spot[:-by], spot[by:])))  14.8 us
    dot_general x3, matrix products, project(): jnp.dot(rows, merged, preferred_element_type=jnp.float32)  12.1 us
  transfers between devices with their start and end apart: 7, of which 6 were waited for; matrix products, arithmetic and copies ran while one was open for 5% of the time, Pallas kernels for 0%

profile of v4, /device:TPU:2, one launch (start us, length us, event | category | flops | bytes accessed | tf_op | source)
XLA Modules:
  0.0 394.2 jit_solution(6964120683394825706)
XLA Ops:
  6.6 1.3 fusion.13
  8.0 2.0 fusion.15.refs_0_
  10.0 1.9 pad_maximum_fusion.3.refs_5_
  11.9 1.1 pad_maximum_fusion.1
  13.0 208.5 %spread.1 = (bf16[512,2048]{1,0:T(8,128)(2,1)}, bf16[2048,1024]{1,0:T(8,128)(2,1)}, bf16[2048,1024]{1,0:T(8,128)(2,1)}, bf16[2048,1024]{1,0:T(8,128)(2,1)}, bf16...) custom-call(bf16[128,2048]{1,0:T(8,128)(2,1)} %fusion.15.refs_0_, ...), custom_call_target="tpu_custom_call" | custom-call | tf_op jit(solution)/shard_map/spread/pallas_call | solution.py:233
  221.5 5.2 %convolution_convert_fusion.2 = bf16[512,1024]{1,0:T(8,128)(2,1)S(1)} fusion(bf16[512,2048]{1,0:T(8,128)(2,1)} %get-tuple-element.12, bf16[2048,1024]{1,0:T(8,128)(2,1)} %get-tuple-element.14), kind=kOutput, calls=%fused_computation.47 | convolution fusion | flops 2148007936 | bytes 7340032 | tf_op jit(solution)/shard_map/dot_general | solution.py:375
  227.7 1.3 fusion.93
  230.0 1.2 copy-done.18
  231.3 4.6 %convolution_convert_fusion.3 = bf16[512,1024]{1,0:T(8,128)(2,1)S(1)} fusion(bf16[512,2048]{1,0:T(8,128)(2,1)S(1)} %copy-done.18, bf16[2048,1024]{1,0:T(8,128)(2,1)} %get-tuple-element.13), kind=kOutput, calls=%fused_computation.48 | convolution fusion | flops 2148007936 | bytes 7340032 | tf_op jit(solution)/shard_map/dot_general | solution.py:375
  235.9 1.0 multiply_cosine_fusion
  238.0 2.6 collective-permute-start
  240.7 2.4 convolution_convert_fusion
  243.4 3.7 collective-permute-start.4
  248.2 1.2 fusion.95
  249.4 2.0 constant_dynamic-slice_fusion
  251.7 1.1 collective-permute-done
  252.8 4.4 %collective-permute-start.1 = (bf16[2,256,512]{2,1,0:T(8,128)(2,1)S(1)}, bf16[2,256,512]{2,1,0:T(8,128)(2,1)S(1)}, u32[]{:S(2)}, u32[]{:S(2)}) collective-permute-start(bf16[2,256,512]{2,1,0:T(8,128)(2,1)S(1)} %collective-permute-done), channel_id=1, source_target_pairs={{0,4},{4,1},{1,5},{5,2},{2,6},{6,3},{3,7},{8,12},{12,9},{9,13},{13... | collective-permute-start | bytes 1572872 | tf_op jit(solution)/shard_map/ppermute | solution.py:33
  257.8 1.3 dynamic_slice.11
  259.1 1.3 dynamic_slice.10
  260.6 4.1 %fusion.9 = f32[2,512,512]{2,1,0:T(8,128)} fusion(f32[512,512]{1,0:T(8,128)S(1)} %fusion.26, f32[2]{0:T(128)} %copy-done.16, pred[512,512]{1,0:T(8,128)(4,1)S(1)} %fusion.27, bf16[64,2,8,512]{3,2,1,0:T(8,128)(2,1)} %bitcast.87, bf16[512,2,128]{2,0,1:T(8,128)(2,1)S(1)} %get-tuple-element.31, bf16[512,2,128]{2,0,1:T(8,128)(2,1)S(1)} %get-tuple-element.32, ...), kind=kOutput, calls=%fused_computation.49 | convolution fusion | flops 809238528 | bytes 6029320 | tf_op jit(solution)/shard_map/hij,jhe->ihe/dot_general | solution.py:302
  264.8 3.9 collective-permute-done.1
  269.6 2.9 collective-permute-start.2
  272.5 5.7 %fusion.92 = (f32[512]{0:T(512)S(1)}, f32[512,512]{1,0:T(8,128)S(1)}) fusion(f32[512]{0:T(512)S(1)} %bitcast.67, bf16[512,512]{1,0:T(8,128)(2,1)S(1)} %multiply_convert_fusion.1, f32[512]{0:T(512)S(1)} %bitcast.69, bf16[30,512]{1,0:T(8,128)(2,1)S(1)} %collective-permute-done.4, f32[512]{0:T(512)S(1)} %bitcast.70, f32[512]{0:T(512)S(1)} %bitcast.71, ...), kind=kLoop, calls=%fused_computation.169 | loop fusion | flops 47971840 | bytes 1669120 | tf_op jit(solution)/shard_map/reduce_sum | solution.py:341
  278.2 1.9 collective-permute-done.2
  280.5 1.3 collective-permute-start.3
  282.0 11.7 %collective-permute-done.3 = bf16[2,256,512]{2,1,0:T(8,128)(2,1)S(1)} collective-permute-done((bf16[2,256,512]{2,1,0:T(8,128)(2,1)S(1)}, bf16[2,256,512]{2,1,0:T(8,128)(2,1)S(1)}, u32[]{:S(2)}, u32[]{:S(2)}) %collective-permute-start.3) | collective-permute-done | bytes 524320 | tf_op jit(solution)/shard_map/ppermute | solution.py:33
  295.2 1.8 copy.23
  297.1 11.5 %fusion.37 = f32[512,2048]{1,0:T(8,128)} fusion(bf16[2048,1024]{1,0:T(8,128)(2,1)} %get-tuple-element.16, f32[512,1024]{1,0:T(8,128)} %copy.23, bf16[512,2048]{1,0:T(8,128)(2,1)} %get-tuple-element.12, bf16[2048,1024]{1,0:T(8,128)(2,1)} %get-tuple-element.15), kind=kOutput, calls=%fused_computation.85 | convolution fusion | flops 4299161600 | bytes 16777216 | tf_op jit(solution)/shard_map/dot_general | solution.py:349
  308.5 7.5 %add_convert_fusion = bf16[512,2048]{1,0:T(8,128)(2,1)} fusion(f32[512,2048]{1,0:T(8,128)} %fusion.37, bf16[2048,1024]{1,0:T(8,128)(2,1)} %get-tuple-element.18, f32[512,512]{1,0:T(8,128)S(1)} %get-tuple-element.20, bf16[512,2048]{1,0:T(8,128)(2,1)S(1)} %copy-done.19, f32[512]{0:T(512)S(1)} %copy-done.12, f32[512]{0:T(512)S(1)} %copy-done.13, ...), kind=kOutput, calls=%fused_computation.29 | convolution fusion | flops 2153775104 | bytes 13639680 | tf_op jit(solution)/shard_map/dot_general | solution.py:349
  316.1 42.7 %reduce-scatter.2.cloned.1.call-done = bf16[128,2048]{1,0:T(8,128)(2,1)} async-done(((bf16[512,2048]{1,0:T(8,128)(2,1)}), bf16[128,2048]{1,0:T(8,128)(2,1)}) %reduce-scatter.2.cloned.1.call-update) | async-done | bytes 524304 | tf_op jit(solution)/shard_map/reduce_scatter | solution.py:426
  358.8 3.5 collective-permute-start.5
  362.3 24.2 %collective-permute-done.5 = bf16[128,2048]{1,0:T(8,128)(2,1)S(1)} collective-permute-done((bf16[128,2048]{1,0:T(8,128)(2,1)}, bf16[128,2048]{1,0:T(8,128)(2,1)S(1)}, u32[]{:S(2)}, u32[]{:S(2)}) %collective-permute-start.5) | collective-permute-done | bytes 524320 | tf_op jit(solution)/shard_map/ppermute | solution.py:27
  (74 shorter events, 9.5 us)
Async XLA Ops:
  6.5 5.3 %copy-start.7 = (bf16[256,512]{1,0:T(8,128)(2,1)S(1)}, bf16[256,512]{1,0:T(8,128)(2,1)}, u32[]{:S(2)}) copy-start(bf16[256,512]{1,0:T(8,128)(2,1)} %param.16) | copy-start | bytes 786436
  6.5 5.3 %copy-start.8 = (bf16[256,512]{1,0:T(8,128)(2,1)S(1)}, bf16[256,512]{1,0:T(8,128)(2,1)}, u32[]{:S(2)}) copy-start(bf16[256,512]{1,0:T(8,128)(2,1)} %param.17) | copy-start | bytes 786436
  6.5 5.3 %copy-start.9 = (bf16[256,512]{1,0:T(8,128)(2,1)S(1)}, bf16[256,512]{1,0:T(8,128)(2,1)}, u32[]{:S(2)}) copy-start(bf16[256,512]{1,0:T(8,128)(2,1)} %param.21) | copy-start | bytes 786436
  6.5 5.3 %copy-start.10 = (bf16[256,512]{1,0:T(8,128)(2,1)S(1)}, bf16[256,512]{1,0:T(8,128)(2,1)}, u32[]{:S(2)}) copy-start(bf16[256,512]{1,0:T(8,128)(2,1)} %param.20) | copy-start | bytes 786436
  6.5 352.2 %reduce-scatter.2.cloned.1.call-start = ((), (), s32[]{:S(2)}) async-start(), calls=%async_computation.1 | async-start | bytes 2621440 | tf_op jit(solution)/shard_map/reduce_scatter | solution.py:426
  7.9 229.0 %copy-start.16 = (f32[2]{0:T(128)}, f32[2]{0:T(128)S(1)}, u32[]{:S(2)}) copy-start(f32[2]{0:T(128)S(1)} %broadcast_multiply_fusion.2) | copy-start | bytes 28
  229.7 1.6 copy-start.18
  231.3 5.7 %copy-start.1 = (f32[512,2,128]{2,1,0:T(2,128)S(1)}, f32[512,2,128]{2,1,0:T(2,128)}, u32[]{:S(2)}) copy-start(f32[512,2,128]{2,1,0:T(2,128)} %get-tuple-element.25) | copy-start | bytes 1572868
  231.3 5.7 %copy-start.2 = (f32[512,2,128]{2,1,0:T(2,128)S(1)}, f32[512,2,128]{2,1,0:T(2,128)}, u32[]{:S(2)}) copy-start(f32[512,2,128]{2,1,0:T(2,128)} %get-tuple-element.26) | copy-start | bytes 1572868
  235.9 1.5 copy-start.20
  237.0 3.6 copy-start.17
  237.3 3.3 copy-start.5
  237.3 3.3 copy-start.6
  237.4 23.3 %copy-start.3 = (bf16[512,2,128]{2,0,1:T(8,128)(2,1)}, bf16[512,2,128]{2,0,1:T(8,128)(2,1)S(1)}, u32[]{:S(2)}) copy-start(bf16[512,2,128]{2,0,1:T(8,128)(2,1)S(1)} %get-tuple-element.32) | copy-start | bytes 786436
  238.0 14.8 %collective-permute-start = (bf16[2,256,512]{2,1,0:T(8,128)(2,1)S(1)}, bf16[2,256,512]{2,1,0:T(8,128)(2,1)S(1)}, u32[]{:S(2)}, u32[]{:S(2)}) collective-permute-start(bf16[2,256,512]{2,1,0:T(8,128)(2,1)S(1)} %convolution_convert_fusion.4), channel_id=1, source_target_pairs={{0,4},{4,1},{1,5},{5,2},{2,6},{6,3},{3,7},{8,12},{12,9},{9,13},{13... | collective-permute-start | bytes 1572872 | tf_op jit(solution)/shard_map/ppermute | solution.py:33
  243.4 29.1 %collective-permute-start.4 = (bf16[30,512]{1,0:T(8,128)(2,1)S(1)}, bf16[30,512]{1,0:T(8,128)(2,1)S(1)}, u32[]{:S(2)}, u32[]{:S(2)}) collective-permute-start(bf16[30,512]{1,0:T(8,128)(2,1)S(1)} %slice.268), channel_id=1, source_target_pairs={{0,4},{4,1},{1,5},{5,2},{2,6},{6,3},{3,7},{8,12},{12,9},{9,13},{13... | collective-permute-start | bytes 92168 | tf_op jit(solution)/shard_map/ppermute | solution.py:33
  252.8 15.9 %collective-permute-start.1 = (bf16[2,256,512]{2,1,0:T(8,128)(2,1)S(1)}, bf16[2,256,512]{2,1,0:T(8,128)(2,1)S(1)}, u32[]{:S(2)}, u32[]{:S(2)}) collective-permute-start(bf16[2,256,512]{2,1,0:T(8,128)(2,1)S(1)} %collective-permute-done), channel_id=1, source_target_pairs={{0,4},{4,1},{1,5},{5,2},{2,6},{6,3},{3,7},{8,12},{12,9},{9,13},{13... | collective-permute-start | bytes 1572872 | tf_op jit(solution)/shard_map/ppermute | solution.py:33
  264.8 15.3 %copy-start.11 = (f32[2]{0:T(128)S(1)}, f32[2]{0:T(128)}, u32[]{:S(2)}) copy-start(f32[2]{0:T(128)} %multiply_exponential_fusion.4) | copy-start | bytes 28
  264.8 15.3 %copy-start.14 = (f32[2]{0:T(128)S(1)}, f32[2]{0:T(128)}, u32[]{:S(2)}) copy-start(f32[2]{0:T(128)} %multiply_exponential_fusion.3) | copy-start | bytes 28
  269.6 10.5 %collective-permute-start.2 = (bf16[2,256,512]{2,1,0:T(8,128)(2,1)S(1)}, bf16[2,256,512]{2,1,0:T(8,128)(2,1)S(1)}, u32[]{:S(2)}, u32[]{:S(2)}) collective-permute-start(bf16[2,256,512]{2,1,0:T(8,128)(2,1)S(1)} %fusion.34), channel_id=1, source_target_pairs={{0,1},{4,5},{1,2},{5,6},{2,3},{6,7},{8,9},{12,13},{9,10},{13,14},{... | collective-permute-start | bytes 1572872 | tf_op jit(solution)/shard_map/ppermute | solution.py:33
  272.5 21.2 %copy-start = (f32[2,512,512]{2,1,0:T(8,128)S(1)}, f32[2,512,512]{2,1,0:T(8,128)}, u32[]{:S(2)}) copy-start(f32[2,512,512]{2,1,0:T(8,128)} %fusion.9) | copy-start | bytes 6291460
  272.5 21.2 %copy-start.4 = (bf16[512,2,128]{2,0,1:T(8,128)(2,1)S(1)}, bf16[512,2,128]{2,0,1:T(8,128)(2,1)}, u32[]{:S(2)}) copy-start(bf16[512,2,128]{2,0,1:T(8,128)(2,1)} %copy-done.3) | copy-start | bytes 786436
  272.5 21.2 %copy-start.15 = (f32[2]{0:T(128)S(1)}, f32[2]{0:T(128)}, u32[]{:S(2)}) copy-start(f32[2]{0:T(128)} %multiply_exponential_fusion.2) | copy-start | bytes 28
  280.5 13.2 %collective-permute-start.3 = (bf16[2,256,512]{2,1,0:T(8,128)(2,1)S(1)}, bf16[2,256,512]{2,1,0:T(8,128)(2,1)S(1)}, u32[]{:S(2)}, u32[]{:S(2)}) collective-permute-start(bf16[2,256,512]{2,1,0:T(8,128)(2,1)S(1)} %fusion.38), channel_id=1, source_target_pairs={{0,2},{4,6},{1,3},{5,7},{8,10},{12,14},{9,11},{13,15},{16,18},{20,... | collective-permute-start | bytes 1572872 | tf_op jit(solution)/shard_map/ppermute | solution.py:33
  297.0 11.5 %copy-start.12 = (f32[512]{0:T(512)S(1)}, f32[512]{0:T(512)}, u32[]{:S(2)}) copy-start(f32[512]{0:T(512)} %dynamic_slice.11) | copy-start | bytes 6148
  297.0 11.5 %copy-start.13 = (f32[512]{0:T(512)S(1)}, f32[512]{0:T(512)}, u32[]{:S(2)}) copy-start(f32[512]{0:T(512)} %dynamic_slice.10) | copy-start | bytes 6148
  297.0 11.5 %copy-start.19 = (bf16[512,2048]{1,0:T(8,128)(2,1)S(1)}, bf16[512,2048]{1,0:T(8,128)(2,1)}, u32[]{:S(2)}) copy-start(bf16[512,2048]{1,0:T(8,128)(2,1)} %get-tuple-element.12) | copy-start | bytes 6291460
  358.8 27.8 %collective-permute-start.5 = (bf16[128,2048]{1,0:T(8,128)(2,1)}, bf16[128,2048]{1,0:T(8,128)(2,1)S(1)}, u32[]{:S(2)}, u32[]{:S(2)}) collective-permute-start(bf16[128,2048]{1,0:T(8,128)(2,1)} %reduce-scatter.2.cloned.1.call-done), channel_id=1, source_target_pairs={{0,0},{1,8},{2,16},{3,24},{8,1},{9,9},{10,17},{11,25},{16,2},{17,1... | collective-permute-start | bytes 1572872 | tf_op jit(solution)/shard_map/ppermute | solution.py:27
Sparse Core Ops, SparseCore 0:
  316.2 42.5 reduce-scatter.1

commit v5 on v3

--- a/solution.py
+++ b/solution.py
@@ -173,11 +173,14 @@
         landed(k, core, lo, other_held)
         push(k, core, lo, other_held, 9, beside)
         push(k, core, lo, other_held, 10, sibling)
+        landed(k, core + 2, lo, other_held)
+        if k < count - 1:
+            push(k, core + 2, lo, other_held, 11, beside)
+        push(k, core + 2, lo, other_held, 12, sibling)
         landed(k, core + 2, 1 - lo, held)
-        push(k, core + 2, 1 - lo, held, 11, across)
-        push(k, core + 2, 1 - lo, held, 12, sibling)
-        landed(k, core + 2, lo, other_held)
-        push(k, core + 2, lo, other_held, 13, sibling)
+        if k == count - 1:
+            push(k, core + 2, 1 - lo, held, 11, across)
+        push(k, core + 2, 1 - lo, held, 13, sibling)
         landed(k, core, 1 - lo, held)
         push(k, core, 1 - lo, held, 14, sibling)
 

time: 373 us -> 393 us (1.054)
  Pallas kernels: 179 us -> 205 us
  waiting for transfers between devices: 89.9 us -> 85.4 us
    pallas_call x1, Pallas kernels: 179 us -> 205 us  [spread(): pl.pallas_call(lambda *refs: spread_kernel(count, *refs), out_shape=outs,...]
    reduce_scatter x1, waiting for transfers between devices: 52.8 us -> 48.5 us  [local(): lax.psum_scatter(mixed, 'hi', scatter_dimension=0, tiled=True)]
where the time goes in v5:
time: 393 us
  Pallas kernels  205 us (52%)
  waiting for transfers between devices  85.4 us (22%)
  matrix products  32.6 us (8%)
  other arithmetic  25.8 us (7%)
  starting transfers between devices  17.7 us (5%)
  between operations  13.8 us (4%)
  local copies, waits for them, and re-layouts  12.4 us (3%)
    pallas_call x1, Pallas kernels, spread(): pl.pallas_call(lambda *refs: spread_kernel(count, *refs), out_shape=outs,...  205 us
    reduce_scatter x1, waiting for transfers between devices, local(): lax.psum_scatter(mixed, 'hi', scatter_dimension=0, tiled=True)  48.5 us
    ppermute x1, waiting for transfers between devices, swap_planes(): return lax.ppermute(x, ('hi', 'tp'), pairs)  24.3 us
    dot_general x2, matrix products, project(): jnp.dot(rows, merged, preferred_element_type=jnp.float32)  19.4 us
    ppermute x5, starting transfers between devices, from_behind(): return lax.ppermute(x, ('lo', 'tp'), list(zip(spot[:-by], spot[by:])))  14.1 us
    ppermute x5, waiting for transfers between devices, from_behind(): return lax.ppermute(x, ('lo', 'tp'), list(zip(spot[:-by], spot[by:])))  12.7 us
  transfers between devices with their start and end apart: 7, of which 5 were waited for; matrix products, arithmetic and copies ran while one was open for 9% of the time, Pallas kernels for 0%

profile of v5, /device:TPU:2, one launch (start us, length us, event | category | flops | bytes accessed | tf_op | source)
XLA Modules:
  0.0 392.6 jit_solution(5685555758191577644)
XLA Ops:
  6.6 1.3 fusion.10
  8.0 2.2 pad_maximum_fusion.2.refs_3_
  10.2 1.0 fusion.12.refs_0_
  11.2 1.1 pad_maximum_fusion.1.refs_1_
  12.3 1.1 pad_maximum_fusion.refs_2_
  13.5 204.8 %spread.1 = (bf16[512,2048]{1,0:T(8,128)(2,1)}, bf16[2048,2048]{1,0:T(8,128)(2,1)}, bf16[2048,2560]{1,0:T(8,128)(2,1)}, bf16[2048,1536]{1,0:T(8,128)(2,1)}, bf16...) custom-call(bf16[128,2048]{1,0:T(8,128)(2,1)} %fusion.12.refs_0_, ...), custom_call_target="tpu_custom_call" | custom-call | tf_op jit(solution)/shard_map/spread/pallas_call | solution.py:233
  218.2 8.5 %convolution_convert_fusion.2 = bf16[512,2048]{1,0:T(8,128)(2,1)S(1)} fusion(bf16[512,2048]{1,0:T(8,128)(2,1)} %get-tuple-element.9, bf16[2048,2048]{1,0:T(8,128)(2,1)} %get-tuple-element.10), kind=kOutput, calls=%fused_computation.31 | convolution fusion | flops 4296015872 | bytes 12582912 | tf_op jit(solution)/shard_map/dot_general | solution.py:375
  227.0 1.1 split.28
  230.2 1.0 multiply_cosine_fusion
  233.2 2.4 collective-permute-start
  235.7 10.9 %convolution_convert_fusion = bf16[512,2560]{1,0:T(8,128)(2,1)} fusion(bf16[512,2048]{1,0:T(8,128)(2,1)S(1)} %copy-done.20, bf16[2048,2560]{1,0:T(8,128)(2,1)} %get-tuple-element.11), kind=kOutput, calls=%fused_computation.29 | convolution fusion | flops 5370019840 | bytes 15204352 | tf_op jit(solution)/shard_map/dot_general | solution.py:375
  246.6 1.5 multiply_convert_fusion.1
  248.2 3.6 collective-permute-start.4
  252.9 1.2 fusion.81
  254.1 1.8 constant_dynamic-slice_fusion
  256.3 2.2 collective-permute-start.1
  259.0 1.3 dynamic_slice.10
  260.3 1.3 dynamic_slice.11
  261.7 1.2 fusion.23
  262.9 4.2 %fusion.9 = f32[2,512,512]{2,1,0:T(8,128)} fusion(f32[512,512]{1,0:T(8,128)} %fusion.23, f32[2]{0:T(128)} %copy-done.19, pred[512,512]{1,0:T(8,128)(4,1)S(1)} %fusion.24, bf16[64,2,8,512]{3,2,1,0:T(8,128)(2,1)S(1)} %bitcast.51, bf16[512,2,128]{2,0,1:T(8,128)(2,1)S(1)} %get-tuple-element.25, bf16[512,2,128]{2,0,1:T(8,128)(2,1)S(1)} %get-tuple-element.26, ...), kind=kOutput, calls=%fused_computation.47 | convolution fusion | flops 809238528 | bytes 6029320 | tf_op jit(solution)/shard_map/hij,jhe->ihe/dot_general | solution.py:302
  267.0 1.4 collective-permute-done.1
  269.3 4.5 %collective-permute-start.2 = (bf16[2,256,512]{2,1,0:T(8,128)(2,1)S(1)}, bf16[2,256,512]{2,1,0:T(8,128)(2,1)S(1)}, u32[]{:S(2)}, u32[]{:S(2)}) collective-permute-start(bf16[2,256,512]{2,1,0:T(8,128)(2,1)S(1)} %fusion.27), channel_id=1, source_target_pairs={{0,1},{4,5},{1,2},{5,6},{2,3},{6,7},{8,9},{12,13},{9,10},{13,14},{... | collective-permute-start | bytes 1572872 | tf_op jit(solution)/shard_map/ppermute | solution.py:33
  273.8 5.6 %fusion.78 = (f32[512]{0:T(512)S(1)}, f32[512,512]{1,0:T(8,128)S(1)}) fusion(f32[512]{0:T(512)S(1)} %bitcast.64, bf16[512,512]{1,0:T(8,128)(2,1)S(1)} %multiply_convert_fusion.1, f32[512]{0:T(512)S(1)} %bitcast.66, bf16[30,512]{1,0:T(8,128)(2,1)S(1)} %collective-permute-done.4, f32[512]{0:T(512)S(1)} %bitcast.67, f32[512]{0:T(512)S(1)} %bitcast.68, ...), kind=kLoop, calls=%fused_computation.159 | loop fusion | flops 47971840 | bytes 1669120 | tf_op jit(solution)/shard_map/reduce_sum | solution.py:341
  280.1 1.4 collective-permute-start.3
  281.6 2.5 fusion.25
  284.1 11.2 %collective-permute-done.3 = bf16[2,256,512]{2,1,0:T(8,128)(2,1)S(1)} collective-permute-done((bf16[2,256,512]{2,1,0:T(8,128)(2,1)S(1)}, bf16[2,256,512]{2,1,0:T(8,128)(2,1)S(1)}, u32[]{:S(2)}, u32[]{:S(2)}) %collective-permute-start.3) | collective-permute-done | bytes 524320 | tf_op jit(solution)/shard_map/ppermute | solution.py:33
  296.8 1.8 copy.23
  298.6 2.6 fusion.5
  301.3 7.4 %convolution_convert_fusion.1 = bf16[512,2048]{1,0:T(8,128)(2,1)} fusion(bf16[2048,1536]{1,0:T(8,128)(2,1)} %get-tuple-element.12, bf16[512,512]{1,0:T(8,128)(2,1)S(1)} %copy-done.5, bf16[512,1024]{1,0:T(8,128)(2,1)S(1)} %fusion.5), kind=kOutput, calls=%fused_computation.30 | convolution fusion | flops 3225419776 | bytes 9961472 | tf_op jit(solution)/shard_map/dot_general | solution.py:349
  308.7 48.5 %reduce-scatter.2.cloned.1.call-done = bf16[128,2048]{1,0:T(8,128)(2,1)} async-done(((bf16[512,2048]{1,0:T(8,128)(2,1)}), bf16[128,2048]{1,0:T(8,128)(2,1)}) %reduce-scatter.2.cloned.1.call-update) | async-done | bytes 524304 | tf_op jit(solution)/shard_map/reduce_scatter | solution.py:417
  357.2 3.5 collective-permute-start.5
  360.7 24.3 %collective-permute-done.5 = bf16[128,2048]{1,0:T(8,128)(2,1)S(1)} collective-permute-done((bf16[128,2048]{1,0:T(8,128)(2,1)}, bf16[128,2048]{1,0:T(8,128)(2,1)S(1)}, u32[]{:S(2)}, u32[]{:S(2)}) %collective-permute-start.5) | collective-permute-done | bytes 524320 | tf_op jit(solution)/shard_map/ppermute | solution.py:27
  (75 shorter events, 10.2 us)
Async XLA Ops:
  6.5 3.6 copy-start.1
  6.5 3.6 copy-start.13
  6.5 4.6 %copy-start.11 = (bf16[256,512]{1,0:T(8,128)(2,1)S(1)}, bf16[256,512]{1,0:T(8,128)(2,1)}, u32[]{:S(2)}) copy-start(bf16[256,512]{1,0:T(8,128)(2,1)} %param.16) | copy-start | bytes 786436
  6.5 4.6 %copy-start.12 = (bf16[256,512]{1,0:T(8,128)(2,1)S(1)}, bf16[256,512]{1,0:T(8,128)(2,1)}, u32[]{:S(2)}) copy-start(bf16[256,512]{1,0:T(8,128)(2,1)} %param.17) | copy-start | bytes 786436
  6.5 4.6 %copy-start.4 = (bf16[256,1024]{1,0:T(8,128)(2,1)S(1)}, bf16[256,1024]{1,0:T(8,128)(2,1)}, u32[]{:S(2)}) copy-start(bf16[256,1024]{1,0:T(8,128)(2,1)} %param.18) | copy-start | bytes 1572868
  6.5 350.6 %reduce-scatter.2.cloned.1.call-start = ((), (), s32[]{:S(2)}) async-start(), calls=%async_computation.1 | async-start | bytes 2621440 | tf_op jit(solution)/shard_map/reduce_scatter | solution.py:417
  8.0 4.3 %copy-start.3 = (bf16[256,1024]{1,0:T(8,128)(2,1)S(1)}, bf16[256,1024]{1,0:T(8,128)(2,1)}, u32[]{:S(2)}) copy-start(bf16[256,1024]{1,0:T(8,128)(2,1)} %param.19) | copy-start | bytes 1572868
  8.0 4.3 %copy-start.8 = (bf16[256,512]{1,0:T(8,128)(2,1)S(1)}, bf16[256,512]{1,0:T(8,128)(2,1)}, u32[]{:S(2)}) copy-start(bf16[256,512]{1,0:T(8,128)(2,1)} %param.22) | copy-start | bytes 786436
  8.0 4.3 %copy-start.9 = (bf16[256,512]{1,0:T(8,128)(2,1)S(1)}, bf16[256,512]{1,0:T(8,128)(2,1)}, u32[]{:S(2)}) copy-start(bf16[256,512]{1,0:T(8,128)(2,1)} %param.21) | copy-start | bytes 786436
  8.0 4.3 %copy-start.10 = (bf16[256,512]{1,0:T(8,128)(2,1)S(1)}, bf16[256,512]{1,0:T(8,128)(2,1)}, u32[]{:S(2)}) copy-start(bf16[256,512]{1,0:T(8,128)(2,1)} %param.20) | copy-start | bytes 786436
  229.5 1.7 copy-start.19
  231.3 1.2 copy-start.2
  231.7 0.8 copy-start.6
  231.7 1.6 copy-start.7
  231.7 4.0 %copy-start.20 = (bf16[512,2048]{1,0:T(8,128)(2,1)S(1)}, bf16[512,2048]{1,0:T(8,128)(2,1)}, u32[]{:S(2)}) copy-start(bf16[512,2048]{1,0:T(8,128)(2,1)} %get-tuple-element.9) | copy-start | bytes 6291460
  233.2 23.0 %collective-permute-start = (bf16[2,256,512]{2,1,0:T(8,128)(2,1)S(1)}, bf16[2,256,512]{2,1,0:T(8,128)(2,1)S(1)}, u32[]{:S(2)}, u32[]{:S(2)}) collective-permute-start(bf16[2,256,512]{2,1,0:T(8,128)(2,1)S(1)} %convolution_convert_fusion.3), channel_id=1, source_target_pairs={{0,4},{4,1},{1,5},{5,2},{2,6},{6,3},{3,7},{8,12},{12,9},{9,13},{13... | collective-permute-start | bytes 1572872 | tf_op jit(solution)/shard_map/ppermute | solution.py:33
  248.2 25.6 %collective-permute-start.4 = (bf16[30,512]{1,0:T(8,128)(2,1)S(1)}, bf16[30,512]{1,0:T(8,128)(2,1)S(1)}, u32[]{:S(2)}, u32[]{:S(2)}) collective-permute-start(bf16[30,512]{1,0:T(8,128)(2,1)S(1)} %slice.268), channel_id=1, source_target_pairs={{0,4},{4,1},{1,5},{5,2},{2,6},{6,3},{3,7},{8,12},{12,9},{9,13},{13... | collective-permute-start | bytes 92168 | tf_op jit(solution)/shard_map/ppermute | solution.py:33
  256.3 12.2 %collective-permute-start.1 = (bf16[2,256,512]{2,1,0:T(8,128)(2,1)S(1)}, bf16[2,256,512]{2,1,0:T(8,128)(2,1)S(1)}, u32[]{:S(2)}, u32[]{:S(2)}) collective-permute-start(bf16[2,256,512]{2,1,0:T(8,128)(2,1)S(1)} %collective-permute-done), channel_id=1, source_target_pairs={{0,4},{4,1},{1,5},{5,2},{2,6},{6,3},{3,7},{8,12},{12,9},{9,13},{13... | collective-permute-start | bytes 1572872 | tf_op jit(solution)/shard_map/ppermute | solution.py:33
  267.0 12.7 %copy-start.16 = (f32[2]{0:T(128)S(1)}, f32[2]{0:T(128)}, u32[]{:S(2)}) copy-start(f32[2]{0:T(128)} %multiply_exponential_fusion.4) | copy-start | bytes 28
  267.0 12.7 %copy-start.17 = (f32[2]{0:T(128)S(1)}, f32[2]{0:T(128)}, u32[]{:S(2)}) copy-start(f32[2]{0:T(128)} %multiply_exponential_fusion.3) | copy-start | bytes 28
  269.3 10.5 %collective-permute-start.2 = (bf16[2,256,512]{2,1,0:T(8,128)(2,1)S(1)}, bf16[2,256,512]{2,1,0:T(8,128)(2,1)S(1)}, u32[]{:S(2)}, u32[]{:S(2)}) collective-permute-start(bf16[2,256,512]{2,1,0:T(8,128)(2,1)S(1)} %fusion.27), channel_id=1, source_target_pairs={{0,1},{4,5},{1,2},{5,6},{2,3},{6,7},{8,9},{12,13},{9,10},{13,14},{... | collective-permute-start | bytes 1572872 | tf_op jit(solution)/shard_map/ppermute | solution.py:33
  273.8 7.8 %copy-start.14 = (f32[512]{0:T(512)S(1)}, f32[512]{0:T(512)}, u32[]{:S(2)}) copy-start(f32[512]{0:T(512)} %dynamic_slice.10) | copy-start | bytes 6148
  273.8 7.8 %copy-start.15 = (f32[512]{0:T(512)S(1)}, f32[512]{0:T(512)}, u32[]{:S(2)}) copy-start(f32[512]{0:T(512)} %dynamic_slice.11) | copy-start | bytes 6148
  279.7 15.7 %copy-start = (f32[2,512,512]{2,1,0:T(8,128)S(1)}, f32[2,512,512]{2,1,0:T(8,128)}, u32[]{:S(2)}) copy-start(f32[2,512,512]{2,1,0:T(8,128)} %fusion.9) | copy-start | bytes 6291460
  279.7 15.6 %copy-start.18 = (f32[2]{0:T(128)S(1)}, f32[2]{0:T(128)}, u32[]{:S(2)}) copy-start(f32[2]{0:T(128)} %multiply_exponential_fusion.2) | copy-start | bytes 28
  280.1 15.2 %collective-permute-start.3 = (bf16[2,256,512]{2,1,0:T(8,128)(2,1)S(1)}, bf16[2,256,512]{2,1,0:T(8,128)(2,1)S(1)}, u32[]{:S(2)}, u32[]{:S(2)}) collective-permute-start(bf16[2,256,512]{2,1,0:T(8,128)(2,1)S(1)} %fusion.30), channel_id=1, source_target_pairs={{0,2},{4,6},{1,3},{5,7},{8,10},{12,14},{9,11},{13,15},{16,18},{20,... | collective-permute-start | bytes 1572872 | tf_op jit(solution)/shard_map/ppermute | solution.py:33
  298.6 2.6 copy-start.5
  357.2 27.8 %collective-permute-start.5 = (bf16[128,2048]{1,0:T(8,128)(2,1)}, bf16[128,2048]{1,0:T(8,128)(2,1)S(1)}, u32[]{:S(2)}, u32[]{:S(2)}) collective-permute-start(bf16[128,2048]{1,0:T(8,128)(2,1)} %reduce-scatter.2.cloned.1.call-done), channel_id=1, source_target_pairs={{0,0},{1,8},{2,16},{3,24},{8,1},{9,9},{10,17},{11,25},{16,2},{17,1... | collective-permute-start | bytes 1572872 | tf_op jit(solution)/shard_map/ppermute | solution.py:27
Sparse Core Ops, SparseCore 0:
  308.8 48.2 reduce-scatter.1
